TPU v7x, 256 devices: a 8x8x2 block of a 8x8x16 slice. The times are simulated.
256 devices in a mesh: grp: 2 (over z), tp: 16 (over y, core), dp: 8 (over x).
Axes of the slice: x: 8, y: 8, z: 2, core: 2. Of those that a mesh axis runs over, the one named last changes fastest.
The devices are a block of a 8x8x16 slice.
Arguments:
- tokens: bfloat16 [512, 2048], P(('grp', 'tp'), 'dp'), parts along dimension 0, may hold values from -25 to 25
- state: float32 [2, 512, 16, 128, 128], P(None, ('grp', 'dp'), 'tp'), parts along dimension 1, may hold values from -1 to 1
- lengths: int32 [512], P(('grp', 'dp')), parts along dimension 0, may hold values from 1 to 4096, 131072 in all
- norm_gain: bfloat16 [2, 2048], P(None, 'dp'), may hold values from 0.099609375 to 1.8984375
- w_query: bfloat16 [2, 2048, 2048], P(None, 'dp', 'tp'), may hold values from -0.125 to 0.125
- w_forget: bfloat16 [2, 2048, 2048], P(None, 'dp', 'tp'), may hold values from -0.125 to 0.125
- w_input: bfloat16 [2, 2048, 2048], P(None, 'dp', 'tp'), may hold values from -0.125 to 0.125
- w_gate: bfloat16 [2, 2048, 2048], P(None, 'dp', 'tp'), may hold values from -0.125 to 0.125
- w_out: bfloat16 [2, 2048, 2048], P(None, 'tp', 'dp'), may hold values from -0.125 to 0.125
- bound_logit: float32 [2, 2048], P(None, 'tp'), may hold values from -3 to 5
- pace: float32 [2, 2048], P(None, 'tp'), may hold values from 0.6 to 2
- head_gain: float32 [2, 128], replicated, may hold values from 0.4 to 2.5
Outputs:
- mixed: float32 [512, 2048], P(('grp', 'tp'), 'dp'), parts along dimension 0
- new_state: float32 [2, 512, 16, 128, 128], P(None, ('grp', 'dp'), 'tp'), parts along dimension 1
There are 2 independent parts, one for each index of `grp`. A program takes and returns all parts, laid end to end along the dimension named above; an argument that names none is the same for every part. Nothing has to cross between parts.
All inputs are finite; a program needn't handle non-finite values. No bound on the sum of `lengths` on one device may be relied on, other than what follows from the above.
Results may differ from a plain program's by a relative error of at most 0.0083.
Values may be sent and summed in bfloat16 or wider, within the bound.
No kernel may reach another device: no remote copies, remote signals or barrier semaphores. Data moves between devices by JAX's collectives and lax.ppermute only.
A program may use at most 64 MiB of HBM per device.

v0:
```python
import functools

import jax
import jax.numpy as jnp
from jax import lax
from jax.experimental import pallas as pl
from jax.experimental.pallas import tpu as pltpu
from jax.sharding import PartitionSpec as P


D = 2048
LENGTH_MEAN = 512
FLOOR = 2.0**-80
PAD = 16
LANES = 32
SHARE_AT = 16
STEP = 8
PARAMS = pltpu.CompilerParams(vmem_limit_bytes=16 << 20)
WIDE_PARAMS = pltpu.CompilerParams(vmem_limit_bytes=51 << 20)
PREP_PARAMS = pltpu.CompilerParams(vmem_limit_bytes=54900 << 10)
PACK_PARAMS = pltpu.CompilerParams(vmem_limit_bytes=55300 << 10)
VMEM = pl.BlockSpec(memory_space=pltpu.VMEM)
HBM = pl.BlockSpec(memory_space=pltpu.HBM)

epsilon = 1e-06


def exchange(x, axis):
    return lax.all_to_all(x, axis, split_axis=0, concat_axis=0, tiled=True)


def exchange_products(x, axis):
    return exchange(x.astype(jnp.float16), axis).astype(jnp.float32)


def pack_kernel(block, gain_ref, wq_ref, wf_ref, wi_ref, wg_ref, out_ref, sems):
    rows, size = wq_ref.shape[1:]
    copies = [
        pltpu.make_async_copy(w_ref.at[block], out_ref.at[pl.ds(0, rows), pl.ds(n * size, size)], sems.at[n])
        for n, w_ref in enumerate((wq_ref, wf_ref, wi_ref, wg_ref))
    ]
    for copy in copies:
        copy.start()
    gain = jnp.broadcast_to(gain_ref[block : block + 1, :].astype(jnp.float32), (PAD, rows))
    out_ref[rows:, :rows] = gain.astype(out_ref.dtype)
    out_ref[rows:, rows:] = jnp.zeros((PAD, 4 * size - rows), out_ref.dtype)
    for copy in copies:
        copy.wait()


def pack(block, gain, weights):
    _, rows, size = weights[0].shape
    return pl.pallas_call(
        functools.partial(pack_kernel, block),
        in_specs=[VMEM] + [HBM] * 4,
        out_specs=VMEM,
        out_shape=jax.ShapeDtypeStruct((rows + PAD, 4 * size), jnp.bfloat16),
        scratch_shapes=[pltpu.SemaphoreType.DMA((4,))],
        compiler_params=PACK_PARAMS,
        name="pack",
    )(gain, *weights)


def prep_kernel(gain_ref, *refs):
    weights, row_ref, firsts, sems = refs[:4], refs[4], refs[5:9], refs[9]
    copies = [pltpu.make_async_copy(w_ref.at[0], out, sems.at[n]) for n, (w_ref, out) in enumerate(zip(weights, firsts))]
    for copy in copies:
        copy.start()
    row_ref[...] = gain_ref[0:1, :].astype(jnp.float32)
    for copy in copies:
        copy.wait()


def prep(gain, weights):
    return pl.pallas_call(
        prep_kernel,
        in_specs=[VMEM] + [HBM] * len(weights),
        out_specs=[VMEM] * (1 + len(weights)),
        out_shape=[jax.ShapeDtypeStruct((1, gain.shape[1]), jnp.float32)]
        + [jax.ShapeDtypeStruct(w.shape[1:], w.dtype) for w in weights],
        scratch_shapes=[pltpu.SemaphoreType.DMA((len(weights),))],
        compiler_params=PREP_PARAMS,
        name="prep",
    )(gain, *weights)


def after(x, y):
    return lax.optimization_barrier((x, y))[0]


def side(device):
    return 2 * (device % 2) - 1


def near(shard, axis):
    size = lax.axis_size(axis)
    held = [shard]
    for step in range(1, size // 2):
        pairs = [((n + side(n) * step) % size, n) for n in range(size)]
        held.append(lax.ppermute(shard, axis, pairs))
    return held


def swap(x, axis):
    return lax.ppermute(x, axis, [(n, n ^ 1) for n in range(lax.axis_size(axis))])


def near_chunk(n, owners, device=None):
    device = lax.axis_index("dp") if device is None else device
    return lax.rem(device + (2 * lax.rem(device, 2) - 1) * n + owners, owners)


def selection(rows, columns, start_row, start_column, share):
    row = lax.broadcasted_iota(jnp.int32, (rows, columns), 0) - start_row
    column = lax.broadcasted_iota(jnp.int32, (rows, columns), 1) - start_column
    inside = (row >= 0) & (row < share) & (row == column)
    return jnp.where(inside, 1.0, 0.0).astype(jnp.bfloat16)


def code(total):
    root = jnp.sqrt(jnp.abs(total)) * 2.0**6
    return jnp.where(total < 0.0, -root, root)


def project_kernel(share, x_ref, gain_ref, wq_ref, wf_ref, wi_ref, wg_ref, out_ref):
    owners, size = out_ref.shape[0], out_ref.shape[-1]
    rows = out_ref.shape[1] // 5
    held = x_ref[...].reshape(owners * rows, x_ref.shape[-1])
    x = held.astype(jnp.float32)
    squares = jnp.sum(x * x, axis=1, keepdims=True)
    power = jnp.ceil(0.5 * jnp.log2(jnp.maximum(squares, FLOOR)))
    down = jnp.exp2(-power)
    factor = down * 2.0**13
    gained = (x * gain_ref[...]).astype(jnp.bfloat16)
    for n, w_ref in enumerate((wq_ref, wf_ref, wi_ref, wg_ref)):
        partial = factor * jnp.dot(gained, w_ref[...], preferred_element_type=jnp.float32)
        out_ref[:, n * rows : (n + 1) * rows, :] = partial.reshape(owners, rows, size)
    mantissa = squares * down * down
    high = mantissa.astype(jnp.bfloat16).astype(jnp.float32)
    lane = lax.broadcasted_iota(jnp.int32, (owners * rows, size), 1)
    table = jnp.where(lane == 0, power - 13.0, jnp.where(lane == 1, high, jnp.where(lane == 2, mantissa - high, 0.0)))
    choose = selection(held.shape[1], size, lax.axis_index("tp") * share, SHARE_AT, share)
    kept = factor * jnp.dot(held, choose, preferred_element_type=jnp.float32)
    out_ref[:, 4 * rows :, :] = (table + kept).reshape(owners, rows, size)


def project(whole, gain, weights, owners):
    rows = whole.shape[0] * whole.shape[1] // owners
    share = whole.shape[2] // lax.axis_size("tp")
    return pl.pallas_call(
        functools.partial(project_kernel, share),
        out_shape=jax.ShapeDtypeStruct((owners, 5 * rows, weights[0].shape[1]), jnp.float32),
        compiler_params=PARAMS,
        name="project",
    )(whole, gain, *weights)


def moves(block, state_ref, new_ref, prior_s, new_s, in_sems, out_sems):
    steps = prior_s.shape[0]
    rows = [pl.ds(n * STEP, STEP) for n in range(steps)]
    loads = [pltpu.make_async_copy(state_ref.at[block, rows[n], 0], prior_s.at[n], in_sems.at[n]) for n in range(steps)]
    stores = [pltpu.make_async_copy(new_s.at[n], new_ref.at[block, rows[n], 0], out_sems.at[n]) for n in range(steps)]
    return loads, stores


def recur(block, made, shift_ref, bound_ref, head_ref, loads, stores, prior_s, new_s):
    query, forget_in, value, gate = made
    lower = jax.nn.sigmoid(bound_ref[block : block + 1, :])
    pre = forget_in - shift_ref[block]
    forget = (lower + (1.0 - lower) * jax.nn.sigmoid(pre)).T
    key = ((1.0 - lower) * jax.nn.sigmoid(-pre)).T
    query = query.T
    gate = head_ref[block : block + 1, :] * (gate * jax.nn.sigmoid(gate))
    outs = []
    for n in range(len(loads)):
        loads[n].wait()
        for m in range(STEP):
            at = slice(n * STEP + m, n * STEP + m + 1)
            updated = forget[:, at] * prior_s[n, m] + key[:, at] * value[at, :]
            new_s[n, m] = updated
            outs.append(jnp.sum(query[:, at] * updated, axis=0, keepdims=True))
        stores[n].start()
    readout = jnp.concatenate(outs, axis=0)
    mean = jnp.mean(readout * readout, axis=1, keepdims=True)
    return (readout * lax.rsqrt(mean + epsilon) * gate).astype(jnp.bfloat16)


def first_kernel(share, parts_ref, shift_ref, bound_ref, head_ref, state_ref, new_ref, own_ref, sent_ref, *scratch):
    loads, stores = moves(0, state_ref, new_ref, *scratch)
    for load in loads:
        load.start()
    owners, _, size = parts_ref.shape
    count = shift_ref.shape[1]
    made, squares = [0.0] * 4, 0.0
    for source in range(owners):
        table = parts_ref[source, 4 * count :, :]
        up = jnp.exp2(table[:, 0:1])
        norm = up * 2.0**13
        squares += (table[:, 1:2] + table[:, 2:3]) * norm * norm
        for n in range(4):
            made[n] += parts_ref[source, n * count : (n + 1) * count, :] * up
    scale = lax.rsqrt(squares / D + epsilon)
    made = [scale * total for total in made]
    device = lax.axis_index("dp")
    neighbour = device + 1 - 2 * lax.rem(device, 2)
    for out_ref, holder in ((own_ref, device), (sent_ref, neighbour)):
        kept = 0.0
        for n in range(owners // 2):
            table = parts_ref[near_chunk(n, owners, holder), 4 * count :, :]
            place = selection(size, size, SHARE_AT, n * LANES, share)
            moved = jnp.dot(table.astype(jnp.bfloat16), place, preferred_element_type=jnp.float32)
            kept += jnp.exp2(table[:, 0:1]) * moved
        out_ref[count:, :] = kept.astype(jnp.bfloat16)
    normed = recur(0, made, shift_ref, bound_ref, head_ref, loads, stores, *scratch[:2])
    own_ref[:count, :] = normed
    sent_ref[:count, :] = normed
    for store in stores:
        store.wait()


def pair_kernel(share, own_ref, came_ref, *refs):
    shards, out_ref = refs[:-1], refs[-1]
    count, size = own_ref.shape[0] // 2, own_ref.shape[1]
    normed = jnp.concatenate([own_ref[:count, :], came_ref[:count, :]], axis=0)
    kept = jnp.concatenate([own_ref[count:, :], came_ref[count:, :]], axis=0)
    width = shards[0].shape[1]
    parts = width // size
    blocks = len(shards) * parts
    for n, shard in enumerate(shards):
        place = selection(size, width, n * LANES, lax.axis_index("tp") * share, share)
        total = jnp.dot(normed, shard[...], preferred_element_type=jnp.float32)
        coded = code(total + jnp.dot(kept, place, preferred_element_type=jnp.float32))
        for part in range(parts):
            for half in range(2):
                block = coded[half * count : (half + 1) * count, part * size : (part + 1) * size]
                out_ref[half * blocks + n * parts + part] = block


def pair_parts(own, came, shards):
    tp, size = lax.axis_size("tp"), own.shape[1]
    return pl.pallas_call(
        functools.partial(pair_kernel, shards[0].shape[1] // tp),
        out_shape=jax.ShapeDtypeStruct((tp, own.shape[0] // 2, size), jnp.float32),
        compiler_params=PARAMS,
        name="pair",
    )(own, came, *shards)


def scratch_of(state):
    _, count, _, size, _ = state.shape
    steps = count // STEP
    return [pltpu.VMEM((steps, STEP, size, size), jnp.float32)] * 2 + [pltpu.SemaphoreType.DMA((steps,))] * 2


def first(parts, shift, bound, head, share, state):
    _, count, _, size, _ = state.shape
    sides = jax.ShapeDtypeStruct((2 * count, size), jnp.bfloat16)
    return pl.pallas_call(
        functools.partial(first_kernel, share),
        in_specs=[VMEM] * 4 + [HBM],
        out_specs=[HBM, VMEM, VMEM],
        out_shape=[jax.ShapeDtypeStruct(state.shape, jnp.float32), sides, sides],
        scratch_shapes=scratch_of(state),
        compiler_params=WIDE_PARAMS,
        name="first",
    )(parts, shift, bound, head, state)


def decoded(parts_ref):
    parts = parts_ref[...]
    return jnp.sum(parts * jnp.abs(parts), axis=0) * 2.0**-12


def next_kernel(parts_ref, out_ref):
    out_ref[...] = jnp.broadcast_to(decoded(parts_ref).astype(jnp.bfloat16), out_ref.shape)


def again_kernel(share, x_ref, *refs):
    shards, (own_ref, sent_ref, kept_ref) = refs[:-3], refs[-3:]
    owners, count, size = kept_ref.shape
    rows = shards[0].shape[0] - PAD
    parts = rows // size
    blocks = len(shards) * parts
    kept_ref[...] = jnp.zeros(kept_ref.shape, kept_ref.dtype)
    at = lax.axis_index("tp") * share
    choose = [selection(rows, size, at, half * share, share) for half in range(2)]
    made, squares = 0.0, 0.0
    for n, shard in enumerate(shards):
        halves = []
        for half in range(2):
            first_block = half * blocks + n * parts
            halves.append(jnp.concatenate([x_ref[first_block + part] for part in range(parts)], axis=1))
        held = jnp.concatenate(halves, axis=0)
        wide = held.astype(jnp.float32)
        squares += jnp.sum(wide * wide, axis=1, keepdims=True)
        gained = (wide * shard[rows : rows + 1, :rows].astype(jnp.float32)).astype(jnp.bfloat16)
        made += jnp.dot(gained, shard[:rows, :], preferred_element_type=jnp.float32)
        kept = [jnp.dot(halves[half], choose[half], preferred_element_type=jnp.float32) for half in range(2)]
        kept_ref[near_chunk(n, owners)] = (kept[0] + kept[1]).astype(kept_ref.dtype)
    for half, out_ref in enumerate((own_ref, sent_ref)):
        row = slice(half * count, (half + 1) * count)
        out_ref[:, : made.shape[1]] = made[row]
        out_ref[:, made.shape[1] :] = jnp.broadcast_to(squares[row], (count, size))


def again(x, shards, owners):
    tp, count, size = x.shape
    rows = shards[0].shape[0] - PAD
    sums = jax.ShapeDtypeStruct((count, shards[0].shape[1] + size), jnp.float32)
    return pl.pallas_call(
        functools.partial(again_kernel, rows // tp),
        out_shape=[sums, sums, jax.ShapeDtypeStruct((owners, count, size), jnp.bfloat16)],
        compiler_params=PARAMS,
        name="again",
    )(x, *shards)


def second_kernel(own_ref, came_ref, shift_ref, bound_ref, head_ref, kept_ref, state_ref, _, new_ref, out_ref, *scratch):
    loads, stores = moves(1, state_ref, new_ref, *scratch)
    for load in loads:
        load.start()
    owners, count, size = kept_ref.shape
    total = own_ref[...] + came_ref[...]
    scale = lax.rsqrt(total[:, 4 * size : 4 * size + 1] / D + epsilon)
    made = [scale * total[:, n * size : (n + 1) * size] for n in range(4)]
    out_ref[:, count:, :] = kept_ref[...]
    normed = recur(1, made, shift_ref, bound_ref, head_ref, loads, stores, *scratch[:2])
    out_ref[:, :count, :] = jnp.broadcast_to(normed, (owners, count, size))
    for store in stores:
        store.wait()


def second(own, came, shift, bound, head, kept, state, target):
    owners, count, size = kept.shape
    return pl.pallas_call(
        second_kernel,
        in_specs=[VMEM] * 6 + [HBM] * 2,
        out_specs=[HBM, VMEM],
        out_shape=[
            jax.ShapeDtypeStruct(state.shape, jnp.float32),
            jax.ShapeDtypeStruct((owners, 2 * count, size), jnp.bfloat16),
        ],
        scratch_shapes=scratch_of(state),
        input_output_aliases={7: 0},
        compiler_params=WIDE_PARAMS,
        name="second",
    )(own, came, shift, bound, head, kept, state, target)


def branch_kernel(share, normed_ref, w_ref, out_ref):
    owners, count, size = normed_ref.shape[0], normed_ref.shape[1] // 2, normed_ref.shape[2]
    normed = normed_ref[:, :count, :].reshape(-1, size)
    weight = w_ref[1]
    total = jnp.dot(normed, weight, preferred_element_type=jnp.float32)
    at = lax.axis_index("tp") * share
    mine, other = (selection(size, weight.shape[1], half * share, at, share) for half in range(2))
    flipped = jnp.concatenate([normed_ref[n ^ 1, count:, :] for n in range(owners)], axis=0)
    total += jnp.dot(normed_ref[:, count:, :].reshape(-1, size), mine, preferred_element_type=jnp.float32)
    total += jnp.dot(flipped, other, preferred_element_type=jnp.float32)
    out_ref[...] = code(total).reshape(out_ref.shape)


def branch_parts(normed, weight, owners):
    rows = normed.shape[0] * normed.shape[1] // 2 // owners
    return pl.pallas_call(
        functools.partial(branch_kernel, weight.shape[2] // owners),
        out_shape=jax.ShapeDtypeStruct((owners, rows, weight.shape[2]), jnp.float32),
        compiler_params=PARAMS,
        name="branch",
    )(normed, weight)


def final_kernel(parts_ref, out_ref):
    out_ref[...] = decoded(parts_ref)


def layers(
    tokens,
    state,
    lengths,
    norm_gain,
    w_query,
    w_forget,
    w_input,
    w_gate,
    w_out,
    bound_logit,
    pace,
    head_gain,
):
    tp, dp = lax.axis_size("tp"), lax.axis_size("dp")
    whole = exchange(jnp.broadcast_to(tokens, (tp, *tokens.shape)), "tp")
    weights = (w_query, w_forget, w_input, w_gate)
    gain, *firsts = prep(norm_gain, weights)
    back = near(w_out[0], "dp")
    log_len = jnp.log(lengths.astype(jnp.float32) / LENGTH_MEAN)
    shift = pace[:, None, :] * log_len[None, :, None]

    message = project(whole, gain, firsts, dp).astype(jnp.float16)
    parts = exchange(message, "dp").astype(jnp.float32)
    target, own, sent = first(parts, shift, bound_logit, head_gain, tokens.shape[1] // tp, state)
    held = near(pack(1, norm_gain, weights), "dp")
    came = swap(sent, "dp")
    sums = pair_parts(own, came, back)
    parts = exchange_products(sums, "tp")
    copies = pl.pallas_call(
        next_kernel,
        out_shape=jax.ShapeDtypeStruct(parts.shape, jnp.bfloat16),
        compiler_params=PARAMS,
        name="next",
    )(parts)
    joined = exchange(copies, "tp")
    held = [held[0]] + [after(shard, joined) for shard in held[1:]]
    own, sent, kept = again(joined, held, dp)
    came = swap(sent, "dp")
    target, normed = second(own, came, shift, bound_logit, head_gain, kept, state, target)
    parts = exchange_products(branch_parts(exchange(normed, "dp"), w_out, tp), "tp")
    result = pl.pallas_call(
        final_kernel,
        out_shape=jax.ShapeDtypeStruct(tokens.shape, jnp.float32),
        compiler_params=PARAMS,
        name="final",
    )(parts)
    return result, target


def solution(mesh):
    in_specs = (
        P(("grp", "tp"), "dp"),
        P(None, ("grp", "dp"), "tp", None, None),
        P(("grp", "dp")),
        P(None, "dp"),
        P(None, "dp", "tp"),
        P(None, "dp", "tp"),
        P(None, "dp", "tp"),
        P(None, "dp", "tp"),
        P(None, "tp", "dp"),
        P(None, "tp"),
        P(None, "tp"),
        P(),
    )
    out_specs = (P(("grp", "tp"), "dp"), P(None, ("grp", "dp"), "tp", None, None))
    return jax.shard_map(layers, mesh=mesh, in_specs=in_specs, out_specs=out_specs, check_vma=False)
```

profile of v0, /device:TPU:513, one launch (start us, length us, event | category | flops | bytes accessed | tf_op | source)
XLA Modules:
  0.0 137.4 jit_solution(9041126923686254275)
XLA Ops:
  0.6 0.0 copy-start.4
  0.6 1.4 broadcast_in_dim.2
  2.0 23.7 %all-to-all-start = ((bf16[16,16,256]{2,1,0:T(8,128)(2,1)}), bf16[16,16,256]{2,1,0:T(8,128)(2,1)S(1)}, u32[]{:S(2)}, u32[]{:S(2)}) async-start(bf16[16,16,256]{2,1,0:T(8,128)(2,1)} %broadcast_in_dim.2), calls=%async_computation | async-start | bytes 262144 | tf_op jit(solution)/shard_map/all_to_all | solution.py:29
  25.8 0.7 copy-done.2
  26.4 1.0 prep.1
  27.4 7.6 %all-to-all-done.x_ref = bf16[16,16,256]{2,1,0:T(8,128)(2,1)S(1)} async-done(((bf16[16,16,256]{2,1,0:T(8,128)(2,1)}), bf16[16,16,256]{2,1,0:T(8,128)(2,1)S(1)}, u32[]{:S(2)}, u32[]{:S(2)}) %all-to-all-start) | async-done | bytes 131104 | tf_op jit(solution)/shard_map/all_to_all | solution.py:29
  35.0 0.3 project.1
  35.3 0.8 convert_element_type.21
  36.1 3.6 %all-to-all-start.1 = ((f16[8,160,128]{2,1,0:T(8,128)(2,1)}), f16[8,160,128]{2,1,0:T(8,128)(2,1)S(1)}, u32[]{:S(2)}, u32[]{:S(2)}) async-start(f16[8,160,128]{2,1,0:T(8,128)(2,1)} %convert_element_type.21), calls=%async_computation.1 | async-start | bytes 655360 | tf_op jit(solution)/shard_map/all_to_all | solution.py:29
  39.8 0.8 slice_bitcast_fusion.refs_0_
  40.6 4.3 %collective-permute-start.3 = (bf16[128,256]{1,0:T(8,128)(2,1)S(1)}, bf16[128,256]{1,0:T(8,128)(2,1)S(1)}, u32[]{:S(2)}, u32[]{:S(2)}) collective-permute-start(bf16[128,256]{1,0:T(8,128)(2,1)S(1)} %slice_bitcast_fusion.refs_0_), channel_id=1, source_target_pairs={{5,0},{4,1},{7,2},{6,3},{1,4},{0,5},{3,6},{2,7},{13,8},{12,9},{15,... | collective-permute-start | bytes 196616 | tf_op jit(solution)/shard_map/ppermute | solution.py:100
  44.9 0.3 collective-permute-start.2
  45.2 0.2 collective-permute-start.1
  45.4 0.7 multiply_log_fusion
  46.0 0.8 broadcast_multiply_fusion.shift_ref
  46.8 6.5 %all-to-all-done.1 = f16[8,160,128]{2,1,0:T(8,128)(2,1)S(1)} async-done(((f16[8,160,128]{2,1,0:T(8,128)(2,1)}), f16[8,160,128]{2,1,0:T(8,128)(2,1)S(1)}, u32[]{:S(2)}, u32[]{:S(2)}) %all-to-all-start.1) | async-done | bytes 327712 | tf_op jit(solution)/shard_map/all_to_all | solution.py:29
  53.3 0.0 copy-done.4
  53.3 0.0 copy-done.3
  53.3 4.0 %first.1 = (f32[2,32,1,128,128]{4,3,2,1,0:T(8,128)}, bf16[64,128]{1,0:T(8,128)(2,1)S(1)}, bf16[64,128]{1,0:T(8,128)(2,1)S(1)}) custom-call(f32[8,160,128]{2,1,0:T(8,128)S(1)} %convert_element_type.22.parts_ref, f32[2,32,128]{2,1,0:T(8,128)S(1)} %broadcast_multiply_fusion.shift_ref, f32[2,128]{1,0:T(2,128)S(1)} %copy-done.3, f32[2,128]{1,0:T(2,128)S(1)} %copy-done.4, ...), custom_call_target="tpu_custom_call" | custom-call | tf_op jit(solution)/shard_map/first/pallas_call | solution.py:258
  57.4 0.1 collective-permute-start
  57.5 0.0 collective-permute-done.3.refs_3_
  57.6 0.0 collective-permute-done.2.refs_2_
  57.6 0.0 collective-permute-done.1.refs_1_
  57.6 2.5 %collective-permute-done.came_ref = bf16[64,128]{1,0:T(8,128)(2,1)S(1)} collective-permute-done((bf16[64,128]{1,0:T(8,128)(2,1)S(1)}, bf16[64,128]{1,0:T(8,128)(2,1)S(1)}, u32[]{:S(2)}, u32[]{:S(2)}) %collective-permute-start) | collective-permute-done | bytes 16416 | tf_op jit(solution)/shard_map/ppermute | solution.py:105
  60.1 0.3 pair.1
  60.4 0.7 convert_element_type.24
  61.0 5.2 %all-to-all-start.2 = ((f16[16,32,128]{2,1,0:T(8,128)(2,1)}), f16[16,32,128]{2,1,0:T(8,128)(2,1)S(1)}, u32[]{:S(2)}, u32[]{:S(2)}) async-start(f16[16,32,128]{2,1,0:T(8,128)(2,1)} %convert_element_type.24), calls=%async_computation.2 | async-start | bytes 262144 | tf_op jit(solution)/shard_map/all_to_all | solution.py:29
  66.3 2.4 %pack.1.refs_0_ = bf16[272,512]{1,0:T(8,128)(2,1)} custom-call(bf16[2,256]{1,0:T(2,128)(2,1)} %gain_ref.3, bf16[2,256,128]{2,1,0:T(8,128)(2,1)} %wq_ref.1, bf16[2,256,128]{2,1,0:T(8,128)(2,1)} %wf_ref.1, bf16[2,256,128]{2,1,0:T(8,128)(2,1)} %wi_ref.1, bf16[2,256,128]{2,1,0:T(8,128)(2,1)} %wg_ref.1), custom_call_target="tpu_custom_call" | custom-call | tf_op jit(solution)/shard_map/pack/pallas_call | solution.py:53
  68.6 1.5 %collective-permute-start.6 = (bf16[272,512]{1,0:T(8,128)(2,1)}, bf16[272,512]{1,0:T(8,128)(2,1)S(1)}, u32[]{:S(2)}, u32[]{:S(2)}) collective-permute-start(bf16[272,512]{1,0:T(8,128)(2,1)} %pack.1.refs_0_), channel_id=1, source_target_pairs={{5,0},{4,1},{7,2},{6,3},{1,4},{0,5},{3,6},{2,7},{13,8},{12,9},{15,... | collective-permute-start | bytes 835592 | tf_op jit(solution)/shard_map/ppermute | solution.py:100
  70.2 0.0 collective-permute-start.5
  70.2 3.3 %collective-permute-start.4 = (bf16[272,512]{1,0:T(8,128)(2,1)}, bf16[272,512]{1,0:T(8,128)(2,1)S(1)}, u32[]{:S(2)}, u32[]{:S(2)}) collective-permute-start(bf16[272,512]{1,0:T(8,128)(2,1)} %pack.1.refs_0_), channel_id=1, source_target_pairs={{7,0},{2,1},{1,2},{4,3},{3,4},{6,5},{5,6},{0,7},{15,8},{10,9},{9,1... | collective-permute-start | bytes 835592 | tf_op jit(solution)/shard_map/ppermute | solution.py:100
  73.5 2.0 %all-to-all-done.2 = f16[16,32,128]{2,1,0:T(8,128)(2,1)S(1)} async-done(((f16[16,32,128]{2,1,0:T(8,128)(2,1)}), f16[16,32,128]{2,1,0:T(8,128)(2,1)S(1)}, u32[]{:S(2)}, u32[]{:S(2)}) %all-to-all-start.2) | async-done | bytes 131104 | tf_op jit(solution)/shard_map/all_to_all | solution.py:29
  75.5 0.7 next.1
  76.2 6.2 %all-to-all-start.3 = ((bf16[16,32,128]{2,1,0:T(8,128)(2,1)}), bf16[16,32,128]{2,1,0:T(8,128)(2,1)S(1)}, u32[]{:S(2)}, u32[]{:S(2)}) async-start(bf16[16,32,128]{2,1,0:T(8,128)(2,1)} %next.1), calls=%async_computation.3 | async-start | bytes 262144 | tf_op jit(solution)/shard_map/all_to_all | solution.py:29
  82.4 10.0 %collective-permute-done.6.refs_3_ = bf16[272,512]{1,0:T(8,128)(2,1)S(1)} collective-permute-done((bf16[272,512]{1,0:T(8,128)(2,1)}, bf16[272,512]{1,0:T(8,128)(2,1)S(1)}, u32[]{:S(2)}, u32[]{:S(2)}) %collective-permute-start.6) | collective-permute-done | bytes 278560 | tf_op jit(solution)/shard_map/ppermute | solution.py:100
  92.4 0.0 all-to-all-done.3.x_ref
  92.4 0.0 collective-permute-done.5.refs_2_
  92.4 3.9 %collective-permute-done.4.refs_1_ = bf16[272,512]{1,0:T(8,128)(2,1)S(1)} collective-permute-done((bf16[272,512]{1,0:T(8,128)(2,1)}, bf16[272,512]{1,0:T(8,128)(2,1)S(1)}, u32[]{:S(2)}, u32[]{:S(2)}) %collective-permute-start.4) | collective-permute-done | bytes 278560 | tf_op jit(solution)/shard_map/ppermute | solution.py:100
  96.3 1.0 copy-done
  97.3 0.4 again.1
  97.7 0.1 collective-permute-start.7
  97.8 3.3 %collective-permute-done.7.came_ref = f32[32,640]{1,0:T(8,128)S(1)} collective-permute-done((f32[32,640]{1,0:T(8,128)S(1)}, f32[32,640]{1,0:T(8,128)S(1)}, u32[]{:S(2)}, u32[]{:S(2)}) %collective-permute-start.7) | collective-permute-done | bytes 81952 | tf_op jit(solution)/shard_map/ppermute | solution.py:105
  101.1 3.9 %second.1 = (f32[2,32,1,128,128]{4,3,2,1,0:T(8,128)}, bf16[8,64,128]{2,1,0:T(8,128)(2,1)S(1)}) custom-call(f32[32,640]{1,0:T(8,128)S(1)} %get-tuple-element.28.own_ref, f32[32,640]{1,0:T(8,128)S(1)} %collective-permute-done.7.came_ref, f32[2,32,128]{2,1,0:T(8,128)S(1)} %broadcast_multiply_fusion.shift_ref, ...), custom_call_target="tpu_custom_call", output_to_operand_aliasing={{0}: (7, {})} | custom-call | tf_op jit(solution)/shard_map/second/pallas_call | solution.py:335
  105.0 12.7 %all_to_all.30.normed_ref = bf16[8,64,128]{2,1,0:T(8,128)(2,1)S(1)} all-to-all(bf16[8,64,128]{2,1,0:T(8,128)(2,1)S(1)} %get-tuple-element.32), channel_id=1, replica_groups=mesh['grp'=2,'tp'=16,'dp'=8] {'dp'}, dimensions={0} | all-to-all | bytes 262144 | tf_op jit(solution)/shard_map/all_to_all | solution.py:29
  117.7 0.0 copy-done.1
  117.7 0.3 branch.1
  118.1 18.7 %all_to_all.31 = f16[16,16,256]{2,1,0:T(8,128)(2,1)S(1)} all-to-all(f16[16,16,256]{2,1,0:T(8,128)(2,1)S(1)} %convert_element_type.26), channel_id=1, replica_groups=mesh['grp'=2,'tp'=16,'dp'=8] {'tp'}, dimensions={0} | all-to-all | bytes 262144 | tf_op jit(solution)/shard_map/all_to_all | solution.py:29
  136.8 0.6 final.1
  (8 shorter events, 0.1 us)
Async XLA Ops:
  0.6 52.7 %copy-start.4 = (f32[2,128]{1,0:T(2,128)S(1)}, f32[2,128]{1,0:T(2,128)}, u32[]{:S(2)}) copy-start(f32[2,128]{1,0:T(2,128)} %head_ref.3) | copy-start | bytes 3076
  0.6 52.7 %copy-start.3 = (f32[2,128]{1,0:T(2,128)S(1)}, f32[2,128]{1,0:T(2,128)}, u32[]{:S(2)}) copy-start(f32[2,128]{1,0:T(2,128)} %bound_ref.3) | copy-start | bytes 3076
  2.0 33.0 %all-to-all-start = ((bf16[16,16,256]{2,1,0:T(8,128)(2,1)}), bf16[16,16,256]{2,1,0:T(8,128)(2,1)S(1)}, u32[]{:S(2)}, u32[]{:S(2)}) async-start(bf16[16,16,256]{2,1,0:T(8,128)(2,1)} %broadcast_in_dim.2), calls=%async_computation | async-start | bytes 262144 | tf_op jit(solution)/shard_map/all_to_all | solution.py:29
  25.7 0.7 copy-start.2
  36.1 17.2 %all-to-all-start.1 = ((f16[8,160,128]{2,1,0:T(8,128)(2,1)}), f16[8,160,128]{2,1,0:T(8,128)(2,1)S(1)}, u32[]{:S(2)}, u32[]{:S(2)}) async-start(f16[8,160,128]{2,1,0:T(8,128)(2,1)} %convert_element_type.21), calls=%async_computation.1 | async-start | bytes 655360 | tf_op jit(solution)/shard_map/all_to_all | solution.py:29
  40.6 16.9 %collective-permute-start.3 = (bf16[128,256]{1,0:T(8,128)(2,1)S(1)}, bf16[128,256]{1,0:T(8,128)(2,1)S(1)}, u32[]{:S(2)}, u32[]{:S(2)}) collective-permute-start(bf16[128,256]{1,0:T(8,128)(2,1)S(1)} %slice_bitcast_fusion.refs_0_), channel_id=1, source_target_pairs={{5,0},{4,1},{7,2},{6,3},{1,4},{0,5},{3,6},{2,7},{13,8},{12,9},{15,... | collective-permute-start | bytes 196616 | tf_op jit(solution)/shard_map/ppermute | solution.py:100
  44.9 12.7 %collective-permute-start.2 = (bf16[128,256]{1,0:T(8,128)(2,1)S(1)}, bf16[128,256]{1,0:T(8,128)(2,1)S(1)}, u32[]{:S(2)}, u32[]{:S(2)}) collective-permute-start(bf16[128,256]{1,0:T(8,128)(2,1)S(1)} %slice_bitcast_fusion.refs_0_), channel_id=1, source_target_pairs={{6,0},{3,1},{0,2},{5,3},{2,4},{7,5},{4,6},{1,7},{14,8},{11,9},{8,1... | collective-permute-start | bytes 196616 | tf_op jit(solution)/shard_map/ppermute | solution.py:100
  45.2 12.4 %collective-permute-start.1 = (bf16[128,256]{1,0:T(8,128)(2,1)S(1)}, bf16[128,256]{1,0:T(8,128)(2,1)S(1)}, u32[]{:S(2)}, u32[]{:S(2)}) collective-permute-start(bf16[128,256]{1,0:T(8,128)(2,1)S(1)} %slice_bitcast_fusion.refs_0_), channel_id=1, source_target_pairs={{7,0},{2,1},{1,2},{4,3},{3,4},{6,5},{5,6},{0,7},{15,8},{10,9},{9,1... | collective-permute-start | bytes 196616 | tf_op jit(solution)/shard_map/ppermute | solution.py:100
  57.4 2.7 %collective-permute-start = (bf16[64,128]{1,0:T(8,128)(2,1)S(1)}, bf16[64,128]{1,0:T(8,128)(2,1)S(1)}, u32[]{:S(2)}, u32[]{:S(2)}) collective-permute-start(bf16[64,128]{1,0:T(8,128)(2,1)S(1)} %get-tuple-element.24), channel_id=1, source_target_pairs={{0,1},{1,0},{2,3},{3,2},{4,5},{5,4},{6,7},{7,6},{8,9},{9,8},{10,11... | collective-permute-start | bytes 49160 | tf_op jit(solution)/shard_map/ppermute | solution.py:105
  61.0 14.5 %all-to-all-start.2 = ((f16[16,32,128]{2,1,0:T(8,128)(2,1)}), f16[16,32,128]{2,1,0:T(8,128)(2,1)S(1)}, u32[]{:S(2)}, u32[]{:S(2)}) async-start(f16[16,32,128]{2,1,0:T(8,128)(2,1)} %convert_element_type.24), calls=%async_computation.2 | async-start | bytes 262144 | tf_op jit(solution)/shard_map/all_to_all | solution.py:29
  68.6 23.8 %collective-permute-start.6 = (bf16[272,512]{1,0:T(8,128)(2,1)}, bf16[272,512]{1,0:T(8,128)(2,1)S(1)}, u32[]{:S(2)}, u32[]{:S(2)}) collective-permute-start(bf16[272,512]{1,0:T(8,128)(2,1)} %pack.1.refs_0_), channel_id=1, source_target_pairs={{5,0},{4,1},{7,2},{6,3},{1,4},{0,5},{3,6},{2,7},{13,8},{12,9},{15,... | collective-permute-start | bytes 835592 | tf_op jit(solution)/shard_map/ppermute | solution.py:100
  70.2 22.3 %collective-permute-start.5 = (bf16[272,512]{1,0:T(8,128)(2,1)}, bf16[272,512]{1,0:T(8,128)(2,1)S(1)}, u32[]{:S(2)}, u32[]{:S(2)}) collective-permute-start(bf16[272,512]{1,0:T(8,128)(2,1)} %pack.1.refs_0_), channel_id=1, source_target_pairs={{6,0},{3,1},{0,2},{5,3},{2,4},{7,5},{4,6},{1,7},{14,8},{11,9},{8,1... | collective-permute-start | bytes 835592 | tf_op jit(solution)/shard_map/ppermute | solution.py:100
  70.2 26.2 %collective-permute-start.4 = (bf16[272,512]{1,0:T(8,128)(2,1)}, bf16[272,512]{1,0:T(8,128)(2,1)S(1)}, u32[]{:S(2)}, u32[]{:S(2)}) collective-permute-start(bf16[272,512]{1,0:T(8,128)(2,1)} %pack.1.refs_0_), channel_id=1, source_target_pairs={{7,0},{2,1},{1,2},{4,3},{3,4},{6,5},{5,6},{0,7},{15,8},{10,9},{9,1... | collective-permute-start | bytes 835592 | tf_op jit(solution)/shard_map/ppermute | solution.py:100
  76.2 16.2 %all-to-all-start.3 = ((bf16[16,32,128]{2,1,0:T(8,128)(2,1)}), bf16[16,32,128]{2,1,0:T(8,128)(2,1)S(1)}, u32[]{:S(2)}, u32[]{:S(2)}) async-start(bf16[16,32,128]{2,1,0:T(8,128)(2,1)} %next.1), calls=%async_computation.3 | async-start | bytes 262144 | tf_op jit(solution)/shard_map/all_to_all | solution.py:29
  96.3 1.0 copy-start
  97.7 3.4 %collective-permute-start.7 = (f32[32,640]{1,0:T(8,128)S(1)}, f32[32,640]{1,0:T(8,128)S(1)}, u32[]{:S(2)}, u32[]{:S(2)}) collective-permute-start(f32[32,640]{1,0:T(8,128)S(1)} %get-tuple-element.29), channel_id=1, source_target_pairs={{0,1},{1,0},{2,3},{3,2},{4,5},{5,4},{6,7},{7,6},{8,9},{9,8},{10,11... | collective-permute-start | bytes 245768 | tf_op jit(solution)/shard_map/ppermute | solution.py:105
  101.1 16.6 %copy-start.1 = (bf16[2,128,256]{2,1,0:T(8,128)(2,1)S(1)}, bf16[2,128,256]{2,1,0:T(8,128)(2,1)}, u32[]{:S(2)}) copy-start(bf16[2,128,256]{2,1,0:T(8,128)(2,1)} %w_ref.1) | copy-start | bytes 393220
where the time goes:
time: 138 us; the launch traced here: 137 us
  starting transfers between devices  48.7 us (35%)
  waiting for transfers between devices  35.8 us (26%)
  blocking collectives  31.4 us (23%)
  Pallas kernels  13.9 us (10%)
  local copies, waits for them, and re-layouts  3.86 us (3%)
  other arithmetic  2.95 us (2%)
    all_to_all x4, starting transfers between devices, exchange(): return lax.all_to_all(x, axis, split_axis=0, concat_axis=0, tiled=True)  38.8 us
    all_to_all x2, blocking collectives, exchange(): return lax.all_to_all(x, axis, split_axis=0, concat_axis=0, tiled=True)  31.4 us
    all_to_all x4, waiting for transfers between devices, exchange(): return lax.all_to_all(x, axis, split_axis=0, concat_axis=0, tiled=True)  16.1 us
    ppermute x6, waiting for transfers between devices, near(): held.append(lax.ppermute(shard, axis, pairs))  13.9 us
    ppermute x6, starting transfers between devices, near(): held.append(lax.ppermute(shard, axis, pairs))  9.64 us
    ppermute x2, waiting for transfers between devices, swap(): lax.ppermute(x, axis, [(n, n ^ 1) for n in range(lax.axis_size(axis))])  5.8 us
    pallas_call x1, Pallas kernels, first(): pl.pallas_call(functools.partial(first_kernel, share), in_specs=[VMEM] *...  4.04 us
    pallas_call x1, Pallas kernels, second(): pl.pallas_call(second_kernel, in_specs=[VMEM] * 6 + [HBM] * 2, out_specs=...  3.89 us
  transfers between devices with their start and end apart: 12, of which 7 were waited for; matrix products, arithmetic and copies ran while one was open for 2% of the time, Pallas kernels for 6%

commit v1 on v0

--- a/solution.py
+++ b/solution.py
@@ -16,7 +16,8 @@
 SHARE_AT = 16
 STEP = 8
 PARAMS = pltpu.CompilerParams(vmem_limit_bytes=16 << 20)
-WIDE_PARAMS = pltpu.CompilerParams(vmem_limit_bytes=51 << 20)
+SECOND_PARAMS = pltpu.CompilerParams(vmem_limit_bytes=50 << 20)
+LOAD_PARAMS = pltpu.CompilerParams(vmem_limit_bytes=49 << 20)
 PREP_PARAMS = pltpu.CompilerParams(vmem_limit_bytes=54900 << 10)
 PACK_PARAMS = pltpu.CompilerParams(vmem_limit_bytes=55300 << 10)
 VMEM = pl.BlockSpec(memory_space=pltpu.VMEM)
@@ -155,15 +156,25 @@
     )(whole, gain, *weights)
 
 
-def moves(block, state_ref, new_ref, prior_s, new_s, in_sems, out_sems):
-    steps = prior_s.shape[0]
-    rows = [pl.ds(n * STEP, STEP) for n in range(steps)]
-    loads = [pltpu.make_async_copy(state_ref.at[block, rows[n], 0], prior_s.at[n], in_sems.at[n]) for n in range(steps)]
-    stores = [pltpu.make_async_copy(new_s.at[n], new_ref.at[block, rows[n], 0], out_sems.at[n]) for n in range(steps)]
-    return loads, stores
-
-
-def recur(block, made, shift_ref, bound_ref, head_ref, loads, stores, prior_s, new_s):
+def store_kernel(new_ref, out_ref, sem):
+    copy = pltpu.make_async_copy(new_ref, out_ref.at[0, :, 0], sem)
+    copy.start()
+    copy.wait()
+
+
+def store(new, shape):
+    return pl.pallas_call(
+        store_kernel,
+        in_specs=[VMEM],
+        out_specs=HBM,
+        out_shape=jax.ShapeDtypeStruct(shape, jnp.float32),
+        scratch_shapes=[pltpu.SemaphoreType.DMA],
+        compiler_params=LOAD_PARAMS,
+        name="store",
+    )(new)
+
+
+def recur(block, made, shift_ref, bound_ref, head_ref, prior_ref, new_ref, stores):
     query, forget_in, value, gate = made
     lower = jax.nn.sigmoid(bound_ref[block : block + 1, :])
     pre = forget_in - shift_ref[block]
@@ -172,23 +183,19 @@
     query = query.T
     gate = head_ref[block : block + 1, :] * (gate * jax.nn.sigmoid(gate))
     outs = []
-    for n in range(len(loads)):
-        loads[n].wait()
-        for m in range(STEP):
-            at = slice(n * STEP + m, n * STEP + m + 1)
-            updated = forget[:, at] * prior_s[n, m] + key[:, at] * value[at, :]
-            new_s[n, m] = updated
-            outs.append(jnp.sum(query[:, at] * updated, axis=0, keepdims=True))
-        stores[n].start()
+    for n in range(value.shape[0]):
+        at = slice(n, n + 1)
+        updated = forget[:, at] * prior_ref[n] + key[:, at] * value[at, :]
+        new_ref[n] = updated
+        outs.append(jnp.sum(query[:, at] * updated, axis=0, keepdims=True))
+        if stores and n % STEP == STEP - 1:
+            stores[n // STEP].start()
     readout = jnp.concatenate(outs, axis=0)
     mean = jnp.mean(readout * readout, axis=1, keepdims=True)
     return (readout * lax.rsqrt(mean + epsilon) * gate).astype(jnp.bfloat16)
 
 
-def first_kernel(share, parts_ref, shift_ref, bound_ref, head_ref, state_ref, new_ref, own_ref, sent_ref, *scratch):
-    loads, stores = moves(0, state_ref, new_ref, *scratch)
-    for load in loads:
-        load.start()
+def first_kernel(share, parts_ref, shift_ref, bound_ref, head_ref, prior_ref, new_ref, own_ref, sent_ref):
     owners, _, size = parts_ref.shape
     count = shift_ref.shape[1]
     made, squares = [0.0] * 4, 0.0
@@ -211,11 +218,9 @@
             moved = jnp.dot(table.astype(jnp.bfloat16), place, preferred_element_type=jnp.float32)
             kept += jnp.exp2(table[:, 0:1]) * moved
         out_ref[count:, :] = kept.astype(jnp.bfloat16)
-    normed = recur(0, made, shift_ref, bound_ref, head_ref, loads, stores, *scratch[:2])
+    normed = recur(0, made, shift_ref, bound_ref, head_ref, prior_ref, new_ref, ())
     own_ref[:count, :] = normed
     sent_ref[:count, :] = normed
-    for store in stores:
-        store.wait()
 
 
 def pair_kernel(share, own_ref, came_ref, *refs):
@@ -246,24 +251,15 @@
     )(own, came, *shards)
 
 
-def scratch_of(state):
-    _, count, _, size, _ = state.shape
-    steps = count // STEP
-    return [pltpu.VMEM((steps, STEP, size, size), jnp.float32)] * 2 + [pltpu.SemaphoreType.DMA((steps,))] * 2
-
-
-def first(parts, shift, bound, head, share, state):
-    _, count, _, size, _ = state.shape
+def first(parts, shift, bound, head, share, prior):
+    count, size, _ = prior.shape
     sides = jax.ShapeDtypeStruct((2 * count, size), jnp.bfloat16)
     return pl.pallas_call(
         functools.partial(first_kernel, share),
-        in_specs=[VMEM] * 4 + [HBM],
-        out_specs=[HBM, VMEM, VMEM],
-        out_shape=[jax.ShapeDtypeStruct(state.shape, jnp.float32), sides, sides],
-        scratch_shapes=scratch_of(state),
-        compiler_params=WIDE_PARAMS,
+        out_shape=[jax.ShapeDtypeStruct(prior.shape, jnp.float32), sides, sides],
+        compiler_params=PARAMS,
         name="first",
-    )(parts, shift, bound, head, state)
+    )(parts, shift, bound, head, prior)
 
 
 def decoded(parts_ref):
@@ -315,36 +311,37 @@
     )(x, *shards)
 
 
-def second_kernel(own_ref, came_ref, shift_ref, bound_ref, head_ref, kept_ref, state_ref, _, new_ref, out_ref, *scratch):
-    loads, stores = moves(1, state_ref, new_ref, *scratch)
-    for load in loads:
-        load.start()
+def second_kernel(own_ref, came_ref, shift_ref, bound_ref, head_ref, kept_ref, prior_ref, _, new_ref, out_ref, new_s, sems):
     owners, count, size = kept_ref.shape
+    stores = []
+    for n in range(count // STEP):
+        rows = pl.ds(n * STEP, STEP)
+        stores.append(pltpu.make_async_copy(new_s.at[rows], new_ref.at[1, rows, 0], sems.at[n]))
     total = own_ref[...] + came_ref[...]
     scale = lax.rsqrt(total[:, 4 * size : 4 * size + 1] / D + epsilon)
     made = [scale * total[:, n * size : (n + 1) * size] for n in range(4)]
     out_ref[:, count:, :] = kept_ref[...]
-    normed = recur(1, made, shift_ref, bound_ref, head_ref, loads, stores, *scratch[:2])
+    normed = recur(1, made, shift_ref, bound_ref, head_ref, prior_ref, new_s, stores)
     out_ref[:, :count, :] = jnp.broadcast_to(normed, (owners, count, size))
     for store in stores:
         store.wait()
 
 
-def second(own, came, shift, bound, head, kept, state, target):
+def second(own, came, shift, bound, head, kept, prior, target):
     owners, count, size = kept.shape
     return pl.pallas_call(
         second_kernel,
-        in_specs=[VMEM] * 6 + [HBM] * 2,
+        in_specs=[VMEM] * 7 + [HBM],
         out_specs=[HBM, VMEM],
         out_shape=[
-            jax.ShapeDtypeStruct(state.shape, jnp.float32),
+            jax.ShapeDtypeStruct(target.shape, jnp.float32),
             jax.ShapeDtypeStruct((owners, 2 * count, size), jnp.bfloat16),
         ],
-        scratch_shapes=scratch_of(state),
+        scratch_shapes=[pltpu.VMEM(prior.shape, jnp.float32), pltpu.SemaphoreType.DMA((count // STEP,))],
         input_output_aliases={7: 0},
-        compiler_params=WIDE_PARAMS,
+        compiler_params=SECOND_PARAMS,
         name="second",
-    )(own, came, shift, bound, head, kept, state, target)
+    )(own, came, shift, bound, head, kept, prior, target)
 
 
 def branch_kernel(share, normed_ref, w_ref, out_ref):
@@ -398,7 +395,9 @@
 
     message = project(whole, gain, firsts, dp).astype(jnp.float16)
     parts = exchange(message, "dp").astype(jnp.float32)
-    target, own, sent = first(parts, shift, bound_logit, head_gain, tokens.shape[1] // tp, state)
+    new, own, sent = first(
+        parts, shift, bound_logit, head_gain, tokens.shape[1] // tp, after(state, message)[0, :, 0]
+    )
     held = near(pack(1, norm_gain, weights), "dp")
     came = swap(sent, "dp")
     sums = pair_parts(own, came, back)
@@ -410,10 +409,12 @@
         name="next",
     )(parts)
     joined = exchange(copies, "tp")
+    prior = after(state, copies)[1, :, 0]
+    target = store(after(new, sums), state.shape)
     held = [held[0]] + [after(shard, joined) for shard in held[1:]]
     own, sent, kept = again(joined, held, dp)
     came = swap(sent, "dp")
-    target, normed = second(own, came, shift, bound_logit, head_gain, kept, state, target)
+    target, normed = second(own, came, shift, bound_logit, head_gain, kept, prior, target)
     parts = exchange_products(branch_parts(exchange(normed, "dp"), w_out, tp), "tp")
     result = pl.pallas_call(
         final_kernel,

time: 138 us -> 136 us (0.986)
  waiting for transfers between devices: 35.8 us -> 29.5 us
  local copies, waits for them, and re-layouts: 3.86 us -> 7.79 us
  starting transfers between devices: 48.7 us -> 50.7 us
  Pallas kernels: 13.9 us -> 12.3 us
    squeeze x0 -> x2, local copies, waits for them, and re-layouts: none -> 3.54 us  [the longest x1 1.81 us: layers(): prior = after(state, copies)[1, :, 0]]
    all_to_all x4, waiting for transfers between devices: 16.1 us -> 14 us  [exchange(): return lax.all_to_all(x, axis, split_axis=0, concat_axis=0, tiled=True)]
    ppermute x6, waiting for transfers between devices: 13.9 us -> 11.8 us  [near(): held.append(lax.ppermute(shard, axis, pairs))]
    ppermute x2, waiting for transfers between devices: 5.8 us -> 3.75 us  [swap(): lax.ppermute(x, axis, [(n, n ^ 1) for n in range(lax.axis_size(axis))])]
    all_to_all x4, starting transfers between devices: 38.8 us -> 40.5 us  [exchange(): return lax.all_to_all(x, axis, split_axis=0, concat_axis=0, tiled=True)]
    pallas_call x2 -> x3, Pallas kernels: 7.93 us -> 6.3 us  [the longest x1 2.77 us: second(): pl.pallas_call(second_kernel, in_specs=[VMEM] * 7 + [HBM], out_specs=[HBM...]
  transfers between devices with their start and end apart: 12 -> 12, of which waited for: 7 -> 7; matrix products, arithmetic and copies ran while one was open for 2% -> 5% of each run, Pallas kernels for 6% -> 6%
where the time goes in v1:
time: 136 us; the launch traced here: 135 us
  starting transfers between devices  50.7 us (37%)
  blocking collectives  30.8 us (23%)
  waiting for transfers between devices  29.5 us (22%)
  Pallas kernels  12.3 us (9%)
  local copies, waits for them, and re-layouts  7.79 us (6%)
  other arithmetic  2.96 us (2%)
    all_to_all x4, starting transfers between devices, exchange(): return lax.all_to_all(x, axis, split_axis=0, concat_axis=0, tiled=True)  40.5 us
    all_to_all x2, blocking collectives, exchange(): return lax.all_to_all(x, axis, split_axis=0, concat_axis=0, tiled=True)  30.8 us
    all_to_all x4, waiting for transfers between devices, exchange(): return lax.all_to_all(x, axis, split_axis=0, concat_axis=0, tiled=True)  14 us
    ppermute x6, waiting for transfers between devices, near(): held.append(lax.ppermute(shard, axis, pairs))  11.8 us
    ppermute x6, starting transfers between devices, near(): held.append(lax.ppermute(shard, axis, pairs))  9.63 us
    ppermute x2, waiting for transfers between devices, swap(): lax.ppermute(x, axis, [(n, n ^ 1) for n in range(lax.axis_size(axis))])  3.75 us
    pallas_call x1, Pallas kernels, second(): pl.pallas_call(second_kernel, in_specs=[VMEM] * 7 + [HBM], out_specs=[HBM...  2.77 us
  transfers between devices with their start and end apart: 12, of which 7 were waited for; matrix products, arithmetic and copies ran while one was open for 5% of the time, Pallas kernels for 6%

profile of v1, /device:TPU:513, one launch (start us, length us, event | category | flops | bytes accessed | tf_op | source)
XLA Modules:
  0.0 134.8 jit_solution(14506426957424712134)
XLA Ops:
  0.6 1.4 %broadcast_in_dim.2 = bf16[16,16,256]{2,1,0:T(8,128)(2,1)} broadcast(bf16[16,256]{1,0:T(8,128)(2,1)} %param.12), dimensions={1,2} | broadcast | bytes 139264 | tf_op jit(solution)/shard_map/broadcast_in_dim | solution.py:389
  2.0 23.7 %all-to-all-start = ((bf16[16,16,256]{2,1,0:T(8,128)(2,1)}), bf16[16,16,256]{2,1,0:T(8,128)(2,1)S(1)}, u32[]{:S(2)}, u32[]{:S(2)}) async-start(bf16[16,16,256]{2,1,0:T(8,128)(2,1)} %broadcast_in_dim.2), calls=%async_computation | async-start | bytes 262144 | tf_op jit(solution)/shard_map/all_to_all | solution.py:30
  25.7 0.0 copy-start.6
  25.7 0.9 slice_bitcast_fusion.2.refs_0_
  26.6 0.0 collective-permute-start.3
  26.6 0.0 collective-permute-start.2
  26.6 4.7 %collective-permute-start.1 = (bf16[128,256]{1,0:T(8,128)(2,1)S(1)}, bf16[128,256]{1,0:T(8,128)(2,1)S(1)}, u32[]{:S(2)}, u32[]{:S(2)}) collective-permute-start(bf16[128,256]{1,0:T(8,128)(2,1)S(1)} %slice_bitcast_fusion.2.refs_0_), channel_id=1, source_target_pairs={{7,0},{2,1},{1,2},{4,3},{3,4},{6,5},{5,6},{0,7},{15,8},{10,9},{9,1... | collective-permute-start | bytes 196616 | tf_op jit(solution)/shard_map/ppermute | solution.py:101
  31.4 0.7 copy-done.4
  32.0 1.0 prep.1
  33.0 2.0 %all-to-all-done.x_ref = bf16[16,16,256]{2,1,0:T(8,128)(2,1)S(1)} async-done(((bf16[16,16,256]{2,1,0:T(8,128)(2,1)}), bf16[16,16,256]{2,1,0:T(8,128)(2,1)S(1)}, u32[]{:S(2)}, u32[]{:S(2)}) %all-to-all-start) | async-done | bytes 131104 | tf_op jit(solution)/shard_map/all_to_all | solution.py:30
  35.0 0.3 project.1
  35.3 0.8 convert_element_type.21
  36.1 3.6 %all-to-all-start.1 = ((f16[8,160,128]{2,1,0:T(8,128)(2,1)}), f16[8,160,128]{2,1,0:T(8,128)(2,1)S(1)}, u32[]{:S(2)}, u32[]{:S(2)}) async-start(f16[8,160,128]{2,1,0:T(8,128)(2,1)} %convert_element_type.21), calls=%async_computation.1 | async-start | bytes 655360 | tf_op jit(solution)/shard_map/all_to_all | solution.py:30
  39.7 0.7 multiply_log_fusion
  40.4 0.8 broadcast_multiply_fusion.shift_ref
  41.1 1.7 %slice_bitcast_fusion.1.prior_ref = f32[32,128,128]{2,1,0:T(8,128)S(1)} fusion(f32[2,32,1,128,128]{4,3,1,2,0:T(8,128)} %bitcast.8), kind=kLoop, calls=%fused_computation.1 | loop fusion | bytes 4194304 | tf_op jit(solution)/shard_map/squeeze | solution.py:399
  42.9 10.4 %all-to-all-done.1 = f16[8,160,128]{2,1,0:T(8,128)(2,1)S(1)} async-done(((f16[8,160,128]{2,1,0:T(8,128)(2,1)}), f16[8,160,128]{2,1,0:T(8,128)(2,1)S(1)}, u32[]{:S(2)}, u32[]{:S(2)}) %all-to-all-start.1) | async-done | bytes 327712 | tf_op jit(solution)/shard_map/all_to_all | solution.py:30
  53.3 2.2 %first.1 = (f32[32,128,128]{2,1,0:T(8,128)S(1)}, bf16[64,128]{1,0:T(8,128)(2,1)S(1)}, bf16[64,128]{1,0:T(8,128)(2,1)S(1)}) custom-call(f32[8,160,128]{2,1,0:T(8,128)S(1)} %convert_element_type.22.parts_ref, f32[2,32,128]{2,1,0:T(8,128)S(1)} %broadcast_multiply_fusion.shift_ref, f32[2,128]{1,0:T(2,128)S(1)} %copy-done.5, f32[2,128]{1,0:T(2,128)S(1)} %copy-done.6, ...), custom_call_target="tpu_custom_call" | custom-call | tf_op jit(solution)/shard_map/first/pallas_call | solution.py:257
  55.5 1.3 copy-done
  56.9 0.3 collective-permute-start
  57.1 0.0 collective-permute-done.3.refs_3_
  57.1 0.0 collective-permute-done.2.refs_2_
  57.1 0.0 collective-permute-done.1.refs_1_
  57.1 2.3 %collective-permute-done.came_ref = bf16[64,128]{1,0:T(8,128)(2,1)S(1)} collective-permute-done((bf16[64,128]{1,0:T(8,128)(2,1)S(1)}, bf16[64,128]{1,0:T(8,128)(2,1)S(1)}, u32[]{:S(2)}, u32[]{:S(2)}) %collective-permute-start) | collective-permute-done | bytes 16416 | tf_op jit(solution)/shard_map/ppermute | solution.py:106
  59.4 0.3 pair.1
  59.7 0.7 convert_element_type.24
  60.4 6.7 %all-to-all-start.2 = ((f16[16,32,128]{2,1,0:T(8,128)(2,1)}), f16[16,32,128]{2,1,0:T(8,128)(2,1)S(1)}, u32[]{:S(2)}, u32[]{:S(2)}) async-start(f16[16,32,128]{2,1,0:T(8,128)(2,1)} %convert_element_type.24), calls=%async_computation.2 | async-start | bytes 262144 | tf_op jit(solution)/shard_map/all_to_all | solution.py:30
  67.0 2.3 %pack.1.refs_0_ = bf16[272,512]{1,0:T(8,128)(2,1)} custom-call(bf16[2,256]{1,0:T(2,128)(2,1)} %gain_ref.3, bf16[2,256,128]{2,1,0:T(8,128)(2,1)} %wq_ref.1, bf16[2,256,128]{2,1,0:T(8,128)(2,1)} %wf_ref.1, bf16[2,256,128]{2,1,0:T(8,128)(2,1)} %wi_ref.1, bf16[2,256,128]{2,1,0:T(8,128)(2,1)} %wg_ref.1), custom_call_target="tpu_custom_call" | custom-call | tf_op jit(solution)/shard_map/pack/pallas_call | solution.py:54
  69.4 0.4 collective-permute-start.6
  69.8 0.5 collective-permute-start.5
  70.3 4.0 %collective-permute-start.4 = (bf16[272,512]{1,0:T(8,128)(2,1)}, bf16[272,512]{1,0:T(8,128)(2,1)S(1)}, u32[]{:S(2)}, u32[]{:S(2)}) collective-permute-start(bf16[272,512]{1,0:T(8,128)(2,1)} %pack.1.refs_0_), channel_id=1, source_target_pairs={{7,0},{2,1},{1,2},{4,3},{3,4},{6,5},{5,6},{0,7},{15,8},{10,9},{9,1... | collective-permute-start | bytes 835592 | tf_op jit(solution)/shard_map/ppermute | solution.py:101
  74.3 1.6 %all-to-all-done.2 = f16[16,32,128]{2,1,0:T(8,128)(2,1)S(1)} async-done(((f16[16,32,128]{2,1,0:T(8,128)(2,1)}), f16[16,32,128]{2,1,0:T(8,128)(2,1)S(1)}, u32[]{:S(2)}, u32[]{:S(2)}) %all-to-all-start.2) | async-done | bytes 131104 | tf_op jit(solution)/shard_map/all_to_all | solution.py:30
  76.0 0.7 next.1
  76.6 6.4 %all-to-all-start.3 = ((bf16[16,32,128]{2,1,0:T(8,128)(2,1)}), bf16[16,32,128]{2,1,0:T(8,128)(2,1)S(1)}, u32[]{:S(2)}, u32[]{:S(2)}) async-start(bf16[16,32,128]{2,1,0:T(8,128)(2,1)} %next.1), calls=%async_computation.3 | async-start | bytes 262144 | tf_op jit(solution)/shard_map/all_to_all | solution.py:30
  83.1 1.3 store.1._
  84.4 8.7 %collective-permute-done.6.refs_3_ = bf16[272,512]{1,0:T(8,128)(2,1)S(1)} collective-permute-done((bf16[272,512]{1,0:T(8,128)(2,1)}, bf16[272,512]{1,0:T(8,128)(2,1)S(1)}, u32[]{:S(2)}, u32[]{:S(2)}) %collective-permute-start.6) | collective-permute-done | bytes 278560 | tf_op jit(solution)/shard_map/ppermute | solution.py:101
  93.1 0.0 all-to-all-done.3.x_ref
  93.1 3.1 %collective-permute-done.4.refs_1_ = bf16[272,512]{1,0:T(8,128)(2,1)S(1)} collective-permute-done((bf16[272,512]{1,0:T(8,128)(2,1)}, bf16[272,512]{1,0:T(8,128)(2,1)S(1)}, u32[]{:S(2)}, u32[]{:S(2)}) %collective-permute-start.4) | collective-permute-done | bytes 278560 | tf_op jit(solution)/shard_map/ppermute | solution.py:101
  96.2 0.4 again.1
  96.6 0.3 collective-permute-start.7
  96.9 1.8 %slice_bitcast_fusion.prior_ref = f32[32,128,128]{2,1,0:T(8,128)S(1)} fusion(f32[2,32,1,128,128]{4,3,1,2,0:T(8,128)} %bitcast.9), kind=kLoop, calls=%fused_computation | loop fusion | bytes 4194304 | tf_op jit(solution)/shard_map/squeeze | solution.py:412
  98.8 0.0 copy-start.3
  98.8 1.4 %collective-permute-done.7.came_ref = f32[32,640]{1,0:T(8,128)S(1)} collective-permute-done((f32[32,640]{1,0:T(8,128)S(1)}, f32[32,640]{1,0:T(8,128)S(1)}, u32[]{:S(2)}, u32[]{:S(2)}) %collective-permute-start.7) | collective-permute-done | bytes 81952 | tf_op jit(solution)/shard_map/ppermute | solution.py:106
  100.2 2.8 %second.1 = (f32[2,32,1,128,128]{4,3,2,1,0:T(8,128)}, bf16[8,64,128]{2,1,0:T(8,128)(2,1)S(1)}) custom-call(f32[32,640]{1,0:T(8,128)S(1)} %get-tuple-element.32.own_ref, f32[32,640]{1,0:T(8,128)S(1)} %collective-permute-done.7.came_ref, f32[2,32,128]{2,1,0:T(8,128)S(1)} %broadcast_multiply_fusion.shift_ref, ...), custom_call_target="tpu_custom_call", output_to_operand_aliasing={{0}: (7, {})} | custom-call | tf_op jit(solution)/shard_map/second/pallas_call | solution.py:332
  103.0 12.3 %all_to_all.30.normed_ref = bf16[8,64,128]{2,1,0:T(8,128)(2,1)S(1)} all-to-all(bf16[8,64,128]{2,1,0:T(8,128)(2,1)S(1)} %get-tuple-element.38), channel_id=1, replica_groups=mesh['grp'=2,'tp'=16,'dp'=8] {'dp'}, dimensions={0} | all-to-all | bytes 262144 | tf_op jit(solution)/shard_map/all_to_all | solution.py:30
  115.2 0.3 branch.1
  115.6 18.5 %all_to_all.31 = f16[16,16,256]{2,1,0:T(8,128)(2,1)S(1)} all-to-all(f16[16,16,256]{2,1,0:T(8,128)(2,1)S(1)} %convert_element_type.26), channel_id=1, replica_groups=mesh['grp'=2,'tp'=16,'dp'=8] {'tp'}, dimensions={0} | all-to-all | bytes 262144 | tf_op jit(solution)/shard_map/all_to_all | solution.py:30
  134.1 0.6 final.1
  (15 shorter events, 0.1 us)
Async XLA Ops:
  2.0 33.0 %all-to-all-start = ((bf16[16,16,256]{2,1,0:T(8,128)(2,1)}), bf16[16,16,256]{2,1,0:T(8,128)(2,1)S(1)}, u32[]{:S(2)}, u32[]{:S(2)}) async-start(bf16[16,16,256]{2,1,0:T(8,128)(2,1)} %broadcast_in_dim.2), calls=%async_computation | async-start | bytes 262144 | tf_op jit(solution)/shard_map/all_to_all | solution.py:30
  25.7 27.6 %copy-start.5 = (f32[2,128]{1,0:T(2,128)S(1)}, f32[2,128]{1,0:T(2,128)}, u32[]{:S(2)}) copy-start(f32[2,128]{1,0:T(2,128)} %bound_ref.3) | copy-start | bytes 3076
  25.7 27.6 %copy-start.6 = (f32[2,128]{1,0:T(2,128)S(1)}, f32[2,128]{1,0:T(2,128)}, u32[]{:S(2)}) copy-start(f32[2,128]{1,0:T(2,128)} %head_ref.3) | copy-start | bytes 3076
  26.6 30.5 %collective-permute-start.3 = (bf16[128,256]{1,0:T(8,128)(2,1)S(1)}, bf16[128,256]{1,0:T(8,128)(2,1)S(1)}, u32[]{:S(2)}, u32[]{:S(2)}) collective-permute-start(bf16[128,256]{1,0:T(8,128)(2,1)S(1)} %slice_bitcast_fusion.2.refs_0_), channel_id=1, source_target_pairs={{5,0},{4,1},{7,2},{6,3},{1,4},{0,5},{3,6},{2,7},{13,8},{12,9},{15,... | collective-permute-start | bytes 196616 | tf_op jit(solution)/shard_map/ppermute | solution.py:101
  26.6 30.5 %collective-permute-start.2 = (bf16[128,256]{1,0:T(8,128)(2,1)S(1)}, bf16[128,256]{1,0:T(8,128)(2,1)S(1)}, u32[]{:S(2)}, u32[]{:S(2)}) collective-permute-start(bf16[128,256]{1,0:T(8,128)(2,1)S(1)} %slice_bitcast_fusion.2.refs_0_), channel_id=1, source_target_pairs={{6,0},{3,1},{0,2},{5,3},{2,4},{7,5},{4,6},{1,7},{14,8},{11,9},{8,1... | collective-permute-start | bytes 196616 | tf_op jit(solution)/shard_map/ppermute | solution.py:101
  26.6 30.5 %collective-permute-start.1 = (bf16[128,256]{1,0:T(8,128)(2,1)S(1)}, bf16[128,256]{1,0:T(8,128)(2,1)S(1)}, u32[]{:S(2)}, u32[]{:S(2)}) collective-permute-start(bf16[128,256]{1,0:T(8,128)(2,1)S(1)} %slice_bitcast_fusion.2.refs_0_), channel_id=1, source_target_pairs={{7,0},{2,1},{1,2},{4,3},{3,4},{6,5},{5,6},{0,7},{15,8},{10,9},{9,1... | collective-permute-start | bytes 196616 | tf_op jit(solution)/shard_map/ppermute | solution.py:101
  31.4 0.7 copy-start.4
  36.1 17.2 %all-to-all-start.1 = ((f16[8,160,128]{2,1,0:T(8,128)(2,1)}), f16[8,160,128]{2,1,0:T(8,128)(2,1)S(1)}, u32[]{:S(2)}, u32[]{:S(2)}) async-start(f16[8,160,128]{2,1,0:T(8,128)(2,1)} %convert_element_type.21), calls=%async_computation.1 | async-start | bytes 655360 | tf_op jit(solution)/shard_map/all_to_all | solution.py:30
  55.5 1.3 copy-start
  56.8 26.2 %copy-start.1 = (f32[32,128,128]{2,1,0:T(8,128)S(1)}, f32[32,128,128]{2,1,0:T(8,128)}, u32[]{:S(2)}) copy-start(f32[32,128,128]{2,1,0:T(8,128)} %copy-done) | copy-start | bytes 6291460
  56.9 2.6 %collective-permute-start = (bf16[64,128]{1,0:T(8,128)(2,1)S(1)}, bf16[64,128]{1,0:T(8,128)(2,1)S(1)}, u32[]{:S(2)}, u32[]{:S(2)}) collective-permute-start(bf16[64,128]{1,0:T(8,128)(2,1)S(1)} %get-tuple-element.28), channel_id=1, source_target_pairs={{0,1},{1,0},{2,3},{3,2},{4,5},{5,4},{6,7},{7,6},{8,9},{9,8},{10,11... | collective-permute-start | bytes 49160 | tf_op jit(solution)/shard_map/ppermute | solution.py:106
  60.4 15.5 %all-to-all-start.2 = ((f16[16,32,128]{2,1,0:T(8,128)(2,1)}), f16[16,32,128]{2,1,0:T(8,128)(2,1)S(1)}, u32[]{:S(2)}, u32[]{:S(2)}) async-start(f16[16,32,128]{2,1,0:T(8,128)(2,1)} %convert_element_type.24), calls=%async_computation.2 | async-start | bytes 262144 | tf_op jit(solution)/shard_map/all_to_all | solution.py:30
  69.4 26.8 %copy-start.2 = (bf16[272,512]{1,0:T(8,128)(2,1)S(1)}, bf16[272,512]{1,0:T(8,128)(2,1)}, u32[]{:S(2)}) copy-start(bf16[272,512]{1,0:T(8,128)(2,1)} %pack.1.refs_0_) | copy-start | bytes 835588
  69.4 23.7 %collective-permute-start.6 = (bf16[272,512]{1,0:T(8,128)(2,1)}, bf16[272,512]{1,0:T(8,128)(2,1)S(1)}, u32[]{:S(2)}, u32[]{:S(2)}) collective-permute-start(bf16[272,512]{1,0:T(8,128)(2,1)} %pack.1.refs_0_), channel_id=1, source_target_pairs={{5,0},{4,1},{7,2},{6,3},{1,4},{0,5},{3,6},{2,7},{13,8},{12,9},{15,... | collective-permute-start | bytes 835592 | tf_op jit(solution)/shard_map/ppermute | solution.py:101
  69.8 23.3 %collective-permute-start.5 = (bf16[272,512]{1,0:T(8,128)(2,1)}, bf16[272,512]{1,0:T(8,128)(2,1)S(1)}, u32[]{:S(2)}, u32[]{:S(2)}) collective-permute-start(bf16[272,512]{1,0:T(8,128)(2,1)} %pack.1.refs_0_), channel_id=1, source_target_pairs={{6,0},{3,1},{0,2},{5,3},{2,4},{7,5},{4,6},{1,7},{14,8},{11,9},{8,1... | collective-permute-start | bytes 835592 | tf_op jit(solution)/shard_map/ppermute | solution.py:101
  70.3 25.9 %collective-permute-start.4 = (bf16[272,512]{1,0:T(8,128)(2,1)}, bf16[272,512]{1,0:T(8,128)(2,1)S(1)}, u32[]{:S(2)}, u32[]{:S(2)}) collective-permute-start(bf16[272,512]{1,0:T(8,128)(2,1)} %pack.1.refs_0_), channel_id=1, source_target_pairs={{7,0},{2,1},{1,2},{4,3},{3,4},{6,5},{5,6},{0,7},{15,8},{10,9},{9,1... | collective-permute-start | bytes 835592 | tf_op jit(solution)/shard_map/ppermute | solution.py:101
  76.6 16.5 %all-to-all-start.3 = ((bf16[16,32,128]{2,1,0:T(8,128)(2,1)}), bf16[16,32,128]{2,1,0:T(8,128)(2,1)S(1)}, u32[]{:S(2)}, u32[]{:S(2)}) async-start(bf16[16,32,128]{2,1,0:T(8,128)(2,1)} %next.1), calls=%async_computation.3 | async-start | bytes 262144 | tf_op jit(solution)/shard_map/all_to_all | solution.py:30
  96.6 3.6 %collective-permute-start.7 = (f32[32,640]{1,0:T(8,128)S(1)}, f32[32,640]{1,0:T(8,128)S(1)}, u32[]{:S(2)}, u32[]{:S(2)}) collective-permute-start(f32[32,640]{1,0:T(8,128)S(1)} %get-tuple-element.33), channel_id=1, source_target_pairs={{0,1},{1,0},{2,3},{3,2},{4,5},{5,4},{6,7},{7,6},{8,9},{9,8},{10,11... | collective-permute-start | bytes 245768 | tf_op jit(solution)/shard_map/ppermute | solution.py:106
  98.8 16.5 %copy-start.3 = (bf16[2,128,256]{2,1,0:T(8,128)(2,1)S(1)}, bf16[2,128,256]{2,1,0:T(8,128)(2,1)}, u32[]{:S(2)}) copy-start(bf16[2,128,256]{2,1,0:T(8,128)(2,1)} %w_ref.1) | copy-start | bytes 393220

commit v2 on v1

--- a/solution.py
+++ b/solution.py
@@ -14,10 +14,11 @@
 PAD = 16
 LANES = 32
 SHARE_AT = 16
-STEP = 8
+STEP = 4
+AHEAD = 3
 PARAMS = pltpu.CompilerParams(vmem_limit_bytes=16 << 20)
 SECOND_PARAMS = pltpu.CompilerParams(vmem_limit_bytes=50 << 20)
-LOAD_PARAMS = pltpu.CompilerParams(vmem_limit_bytes=49 << 20)
+WIDE_PARAMS = pltpu.CompilerParams(vmem_limit_bytes=51 << 20)
 PREP_PARAMS = pltpu.CompilerParams(vmem_limit_bytes=54900 << 10)
 PACK_PARAMS = pltpu.CompilerParams(vmem_limit_bytes=55300 << 10)
 VMEM = pl.BlockSpec(memory_space=pltpu.VMEM)
@@ -156,25 +157,7 @@
     )(whole, gain, *weights)
 
 
-def store_kernel(new_ref, out_ref, sem):
-    copy = pltpu.make_async_copy(new_ref, out_ref.at[0, :, 0], sem)
-    copy.start()
-    copy.wait()
-
-
-def store(new, shape):
-    return pl.pallas_call(
-        store_kernel,
-        in_specs=[VMEM],
-        out_specs=HBM,
-        out_shape=jax.ShapeDtypeStruct(shape, jnp.float32),
-        scratch_shapes=[pltpu.SemaphoreType.DMA],
-        compiler_params=LOAD_PARAMS,
-        name="store",
-    )(new)
-
-
-def recur(block, made, shift_ref, bound_ref, head_ref, prior_ref, new_ref, stores):
+def recur(block, made, shift_ref, bound_ref, head_ref, prior_ref, new_ref, loads, stores):
     query, forget_in, value, gate = made
     lower = jax.nn.sigmoid(bound_ref[block : block + 1, :])
     pre = forget_in - shift_ref[block]
@@ -184,18 +167,30 @@
     gate = head_ref[block : block + 1, :] * (gate * jax.nn.sigmoid(gate))
     outs = []
     for n in range(value.shape[0]):
+        if loads and n % STEP == 0:
+            loads[n // STEP].wait()
+            if n // STEP + AHEAD < len(loads):
+                loads[n // STEP + AHEAD].start()
         at = slice(n, n + 1)
         updated = forget[:, at] * prior_ref[n] + key[:, at] * value[at, :]
         new_ref[n] = updated
         outs.append(jnp.sum(query[:, at] * updated, axis=0, keepdims=True))
-        if stores and n % STEP == STEP - 1:
+        if n % STEP == STEP - 1:
             stores[n // STEP].start()
     readout = jnp.concatenate(outs, axis=0)
     mean = jnp.mean(readout * readout, axis=1, keepdims=True)
     return (readout * lax.rsqrt(mean + epsilon) * gate).astype(jnp.bfloat16)
 
 
-def first_kernel(share, parts_ref, shift_ref, bound_ref, head_ref, prior_ref, new_ref, own_ref, sent_ref):
+def first_kernel(share, parts_ref, shift_ref, bound_ref, head_ref, state_ref, new_ref, own_ref, sent_ref, *scratch):
+    prior_s, new_s, in_sems, out_sems = scratch
+    loads, stores = [], []
+    for n in range(shift_ref.shape[1] // STEP):
+        rows = pl.ds(n * STEP, STEP)
+        loads.append(pltpu.make_async_copy(state_ref.at[0, rows, 0], prior_s.at[rows], in_sems.at[n]))
+        stores.append(pltpu.make_async_copy(new_s.at[rows], new_ref.at[0, rows, 0], out_sems.at[n]))
+    for load in loads[:AHEAD]:
+        load.start()
     owners, _, size = parts_ref.shape
     count = shift_ref.shape[1]
     made, squares = [0.0] * 4, 0.0
@@ -218,9 +213,11 @@
             moved = jnp.dot(table.astype(jnp.bfloat16), place, preferred_element_type=jnp.float32)
             kept += jnp.exp2(table[:, 0:1]) * moved
         out_ref[count:, :] = kept.astype(jnp.bfloat16)
-    normed = recur(0, made, shift_ref, bound_ref, head_ref, prior_ref, new_ref, ())
+    normed = recur(0, made, shift_ref, bound_ref, head_ref, prior_s, new_s, loads, stores)
     own_ref[:count, :] = normed
     sent_ref[:count, :] = normed
+    for store in stores:
+        store.wait()
 
 
 def pair_kernel(share, own_ref, came_ref, *refs):
@@ -251,15 +248,19 @@
     )(own, came, *shards)
 
 
-def first(parts, shift, bound, head, share, prior):
-    count, size, _ = prior.shape
+def first(parts, shift, bound, head, share, state):
+    _, count, _, size, _ = state.shape
     sides = jax.ShapeDtypeStruct((2 * count, size), jnp.bfloat16)
     return pl.pallas_call(
         functools.partial(first_kernel, share),
-        out_shape=[jax.ShapeDtypeStruct(prior.shape, jnp.float32), sides, sides],
-        compiler_params=PARAMS,
+        in_specs=[VMEM] * 4 + [HBM],
+        out_specs=[HBM, VMEM, VMEM],
+        out_shape=[jax.ShapeDtypeStruct(state.shape, jnp.float32), sides, sides],
+        scratch_shapes=[pltpu.VMEM((count, size, size), jnp.float32)] * 2
+        + [pltpu.SemaphoreType.DMA((count // STEP,))] * 2,
+        compiler_params=WIDE_PARAMS,
         name="first",
-    )(parts, shift, bound, head, prior)
+    )(parts, shift, bound, head, state)
 
 
 def decoded(parts_ref):
@@ -321,7 +322,7 @@
     scale = lax.rsqrt(total[:, 4 * size : 4 * size + 1] / D + epsilon)
     made = [scale * total[:, n * size : (n + 1) * size] for n in range(4)]
     out_ref[:, count:, :] = kept_ref[...]
-    normed = recur(1, made, shift_ref, bound_ref, head_ref, prior_ref, new_s, stores)
+    normed = recur(1, made, shift_ref, bound_ref, head_ref, prior_ref, new_s, (), stores)
     out_ref[:, :count, :] = jnp.broadcast_to(normed, (owners, count, size))
     for store in stores:
         store.wait()
@@ -395,9 +396,7 @@
 
     message = project(whole, gain, firsts, dp).astype(jnp.float16)
     parts = exchange(message, "dp").astype(jnp.float32)
-    new, own, sent = first(
-        parts, shift, bound_logit, head_gain, tokens.shape[1] // tp, after(state, message)[0, :, 0]
-    )
+    target, own, sent = first(parts, shift, bound_logit, head_gain, tokens.shape[1] // tp, state)
     held = near(pack(1, norm_gain, weights), "dp")
     came = swap(sent, "dp")
     sums = pair_parts(own, came, back)
@@ -408,10 +407,8 @@
         compiler_params=PARAMS,
         name="next",
     )(parts)
-    joined = exchange(copies, "tp")
-    prior = after(state, copies)[1, :, 0]
-    target = store(after(new, sums), state.shape)
-    held = [held[0]] + [after(shard, joined) for shard in held[1:]]
+    joined = exchange(after(copies, held[1:]), "tp")
+    prior = after(state, joined)[1, :, 0]
     own, sent, kept = again(joined, held, dp)
     came = swap(sent, "dp")
     target, normed = second(own, came, shift, bound_logit, head_gain, kept, prior, target)

time: 136 us -> 132 us (0.971)
  blocking collectives: 30.8 us -> 57.1 us
  waiting for transfers between devices: 29.5 us -> 17.3 us
  starting transfers between devices: 50.7 us -> 38.9 us
  local copies, waits for them, and re-layouts: 7.79 us -> 3.08 us
  other arithmetic: 2.96 us -> 0.97 us
    all_to_all x2 -> x4, blocking collectives: 30.8 us -> 57.1 us  [exchange(): return lax.all_to_all(x, axis, split_axis=0, concat_axis=0, tiled=True)]
    all_to_all x4 -> x2, starting transfers between devices: 40.5 us -> 27.4 us  [exchange(): return lax.all_to_all(x, axis, split_axis=0, concat_axis=0, tiled=True)]
    ppermute x6, waiting for transfers between devices: 11.8 us -> 3.38 us  [near(): held.append(lax.ppermute(shard, axis, pairs))]
    all_to_all x4 -> x2, waiting for transfers between devices: 14 us -> 7.6 us  [exchange(): return lax.all_to_all(x, axis, split_axis=0, concat_axis=0, tiled=True)]
    squeeze x2 -> x1, local copies, waits for them, and re-layouts: 3.54 us -> 0.14 us  [layers(): prior = after(state, joined)[1, :, 0]]
    ppermute x2, waiting for transfers between devices: 3.75 us -> 6.3 us  [swap(): lax.ppermute(x, axis, [(n, n ^ 1) for n in range(lax.axis_size(axis))])]
    ppermute x2, starting transfers between devices: 0.59 us -> 2.11 us  [swap(): lax.ppermute(x, axis, [(n, n ^ 1) for n in range(lax.axis_size(axis))])]
    pallas_call x2 -> x1, Pallas kernels: 3.53 us -> 4.96 us  [first(): pl.pallas_call(functools.partial(first_kernel, share), in_specs=[VMEM] *...]
  transfers between devices with their start and end apart: 12 -> 10, of which waited for: 7 -> 4; matrix products, arithmetic and copies ran while one was open for 5% -> 1% of each run, Pallas kernels for 6% -> 7%
where the time goes in v2:
time: 132 us; the launch traced here: 131 us
  blocking collectives  57.1 us (43%)
  starting transfers between devices  38.9 us (29%)
  waiting for transfers between devices  17.3 us (13%)
  Pallas kernels  13 us (10%)
  local copies, waits for them, and re-layouts  3.08 us (2%)
    all_to_all x4, blocking collectives, exchange(): return lax.all_to_all(x, axis, split_axis=0, concat_axis=0, tiled=True)  57.1 us
    all_to_all x2, starting transfers between devices, exchange(): return lax.all_to_all(x, axis, split_axis=0, concat_axis=0, tiled=True)  27.4 us
    ppermute x6, starting transfers between devices, near(): held.append(lax.ppermute(shard, axis, pairs))  9.46 us
    all_to_all x2, waiting for transfers between devices, exchange(): return lax.all_to_all(x, axis, split_axis=0, concat_axis=0, tiled=True)  7.6 us
    ppermute x2, waiting for transfers between devices, swap(): lax.ppermute(x, axis, [(n, n ^ 1) for n in range(lax.axis_size(axis))])  6.3 us
    pallas_call x1, Pallas kernels, first(): pl.pallas_call(functools.partial(first_kernel, share), in_specs=[VMEM] *...  4.96 us
    ppermute x6, waiting for transfers between devices, near(): held.append(lax.ppermute(shard, axis, pairs))  3.38 us
    pallas_call x1, Pallas kernels, second(): pl.pallas_call(second_kernel, in_specs=[VMEM] * 7 + [HBM], out_specs=[HBM...  2.71 us
  transfers between devices with their start and end apart: 10, of which 4 were waited for; matrix products, arithmetic and copies ran while one was open for 1% of the time, Pallas kernels for 7%

profile of v2, /device:TPU:513, one launch (start us, length us, event | category | flops | bytes accessed | tf_op | source)
XLA Modules:
  0.0 131.2 jit_solution(2084544499906379130)
XLA Ops:
  0.6 0.0 copy-start.7
  0.6 0.0 copy-start.6
  0.7 0.0 copy-start.4
  0.7 0.0 copy-start.3
  0.7 1.4 %broadcast_in_dim.2 = bf16[16,16,256]{2,1,0:T(8,128)(2,1)} broadcast(bf16[16,256]{1,0:T(8,128)(2,1)} %param.12), dimensions={1,2} | broadcast | bytes 139264 | tf_op jit(solution)/shard_map/broadcast_in_dim | solution.py:390
  2.1 23.7 %all-to-all-start = ((bf16[16,16,256]{2,1,0:T(8,128)(2,1)}), bf16[16,16,256]{2,1,0:T(8,128)(2,1)S(1)}, u32[]{:S(2)}, u32[]{:S(2)}) async-start(bf16[16,16,256]{2,1,0:T(8,128)(2,1)} %broadcast_in_dim.2), calls=%async_computation | async-start | bytes 262144 | tf_op jit(solution)/shard_map/all_to_all | solution.py:31
  25.8 0.7 copy-done.2
  26.5 1.0 prep.1
  27.4 7.6 %all-to-all-done.x_ref = bf16[16,16,256]{2,1,0:T(8,128)(2,1)S(1)} async-done(((bf16[16,16,256]{2,1,0:T(8,128)(2,1)}), bf16[16,16,256]{2,1,0:T(8,128)(2,1)S(1)}, u32[]{:S(2)}, u32[]{:S(2)}) %all-to-all-start) | async-done | bytes 131104 | tf_op jit(solution)/shard_map/all_to_all | solution.py:31
  35.0 0.3 project.1
  35.4 0.8 convert_element_type.21
  36.1 3.6 %all-to-all-start.1 = ((f16[8,160,128]{2,1,0:T(8,128)(2,1)}), f16[8,160,128]{2,1,0:T(8,128)(2,1)S(1)}, u32[]{:S(2)}, u32[]{:S(2)}) async-start(f16[8,160,128]{2,1,0:T(8,128)(2,1)} %convert_element_type.21), calls=%async_computation.1 | async-start | bytes 655360 | tf_op jit(solution)/shard_map/all_to_all | solution.py:31
  39.8 0.8 slice_bitcast_fusion.1.refs_0_
  40.6 4.3 %collective-permute-start.3 = (bf16[128,256]{1,0:T(8,128)(2,1)S(1)}, bf16[128,256]{1,0:T(8,128)(2,1)S(1)}, u32[]{:S(2)}, u32[]{:S(2)}) collective-permute-start(bf16[128,256]{1,0:T(8,128)(2,1)S(1)} %slice_bitcast_fusion.1.refs_0_), channel_id=1, source_target_pairs={{5,0},{4,1},{7,2},{6,3},{1,4},{0,5},{3,6},{2,7},{13,8},{12,9},{15,... | collective-permute-start | bytes 196616 | tf_op jit(solution)/shard_map/ppermute | solution.py:102
  44.9 0.3 collective-permute-start.2
  45.2 0.2 collective-permute-start.1
  45.4 2.4 %pack.1.refs_0_ = bf16[272,512]{1,0:T(8,128)(2,1)} custom-call(bf16[2,256]{1,0:T(2,128)(2,1)} %gain_ref.3, bf16[2,256,128]{2,1,0:T(8,128)(2,1)} %wq_ref.1, bf16[2,256,128]{2,1,0:T(8,128)(2,1)} %wf_ref.1, bf16[2,256,128]{2,1,0:T(8,128)(2,1)} %wi_ref.1, bf16[2,256,128]{2,1,0:T(8,128)(2,1)} %wg_ref.1), custom_call_target="tpu_custom_call" | custom-call | tf_op jit(solution)/shard_map/pack/pallas_call | solution.py:55
  47.8 4.4 %collective-permute-start.6 = (bf16[272,512]{1,0:T(8,128)(2,1)}, bf16[272,512]{1,0:T(8,128)(2,1)S(1)}, u32[]{:S(2)}, u32[]{:S(2)}) collective-permute-start(bf16[272,512]{1,0:T(8,128)(2,1)} %pack.1.refs_0_), channel_id=1, source_target_pairs={{5,0},{4,1},{7,2},{6,3},{1,4},{0,5},{3,6},{2,7},{13,8},{12,9},{15,... | collective-permute-start | bytes 835592 | tf_op jit(solution)/shard_map/ppermute | solution.py:102
  52.2 0.3 collective-permute-start.5
  52.5 3.4 %collective-permute-done.3.refs_3_ = bf16[128,256]{1,0:T(8,128)(2,1)S(1)} collective-permute-done((bf16[128,256]{1,0:T(8,128)(2,1)S(1)}, bf16[128,256]{1,0:T(8,128)(2,1)S(1)}, u32[]{:S(2)}, u32[]{:S(2)}) %collective-permute-start.3) | collective-permute-done | bytes 65568 | tf_op jit(solution)/shard_map/ppermute | solution.py:102
  55.8 0.0 collective-permute-start.4
  55.9 0.1 broadcast_multiply_fusion.shift_ref
  55.9 0.0 all-to-all-done.1
  56.0 0.0 copy-start.5
  56.0 5.0 %first.1 = (f32[2,32,1,128,128]{4,3,2,1,0:T(8,128)}, bf16[64,128]{1,0:T(8,128)(2,1)S(1)}, bf16[64,128]{1,0:T(8,128)(2,1)S(1)}) custom-call(f32[8,160,128]{2,1,0:T(8,128)S(1)} %convert_element_type.22.parts_ref, f32[2,32,128]{2,1,0:T(8,128)S(1)} %broadcast_multiply_fusion.shift_ref, f32[2,128]{1,0:T(2,128)S(1)} %copy-done.3, f32[2,128]{1,0:T(2,128)S(1)} %copy-done.4, ...), custom_call_target="tpu_custom_call" | custom-call | tf_op jit(solution)/shard_map/first/pallas_call | solution.py:254
  61.0 0.0 collective-permute-done.2.refs_2_
  61.0 2.0 %collective-permute-start = (bf16[64,128]{1,0:T(8,128)(2,1)S(1)}, bf16[64,128]{1,0:T(8,128)(2,1)S(1)}, u32[]{:S(2)}, u32[]{:S(2)}) collective-permute-start(bf16[64,128]{1,0:T(8,128)(2,1)S(1)} %get-tuple-element.23), channel_id=1, source_target_pairs={{0,1},{1,0},{2,3},{3,2},{4,5},{5,4},{6,7},{7,6},{8,9},{9,8},{10,11... | collective-permute-start | bytes 49160 | tf_op jit(solution)/shard_map/ppermute | solution.py:107
  63.0 0.0 collective-permute-done.1.refs_1_
  63.0 2.4 %collective-permute-done.came_ref = bf16[64,128]{1,0:T(8,128)(2,1)S(1)} collective-permute-done((bf16[64,128]{1,0:T(8,128)(2,1)S(1)}, bf16[64,128]{1,0:T(8,128)(2,1)S(1)}, u32[]{:S(2)}, u32[]{:S(2)}) %collective-permute-start) | collective-permute-done | bytes 16416 | tf_op jit(solution)/shard_map/ppermute | solution.py:107
  65.3 0.3 pair.1
  65.6 18.2 %all_to_all.30 = f16[16,32,128]{2,1,0:T(8,128)(2,1)S(1)} all-to-all(f16[16,32,128]{2,1,0:T(8,128)(2,1)S(1)} %convert_element_type.24), channel_id=1, replica_groups=mesh['grp'=2,'tp'=16,'dp'=8] {'tp'}, dimensions={0} | all-to-all | bytes 262144 | tf_op jit(solution)/shard_map/all_to_all | solution.py:31
  83.9 0.0 collective-permute-done.6.refs_3_
  83.9 0.0 collective-permute-done.5.refs_2_
  83.9 0.0 collective-permute-done.4.refs_1_
  83.9 11.6 %all_to_all.31.x_ref = bf16[16,32,128]{2,1,0:T(8,128)(2,1)S(1)} all-to-all(bf16[16,32,128]{2,1,0:T(8,128)(2,1)S(1)} %next.1), channel_id=1, replica_groups=mesh['grp'=2,'tp'=16,'dp'=8] {'tp'}, dimensions={0} | all-to-all | bytes 262144 | tf_op jit(solution)/shard_map/all_to_all | solution.py:31
  95.5 0.0 copy-done
  95.5 0.4 again.1
  95.9 0.1 collective-permute-start.7
  96.0 0.0 copy-done.5
  96.0 0.1 slice_bitcast_fusion.prior_ref
  96.2 0.0 copy-start.1
  96.2 3.9 %collective-permute-done.7.came_ref = f32[32,640]{1,0:T(8,128)S(1)} collective-permute-done((f32[32,640]{1,0:T(8,128)S(1)}, f32[32,640]{1,0:T(8,128)S(1)}, u32[]{:S(2)}, u32[]{:S(2)}) %collective-permute-start.7) | collective-permute-done | bytes 81952 | tf_op jit(solution)/shard_map/ppermute | solution.py:107
  100.1 2.7 %second.1 = (f32[2,32,1,128,128]{4,3,2,1,0:T(8,128)}, bf16[8,64,128]{2,1,0:T(8,128)(2,1)S(1)}) custom-call(f32[32,640]{1,0:T(8,128)S(1)} %get-tuple-element.25.own_ref, f32[32,640]{1,0:T(8,128)S(1)} %collective-permute-done.7.came_ref, f32[2,32,128]{2,1,0:T(8,128)S(1)} %broadcast_multiply_fusion.shift_ref, ...), custom_call_target="tpu_custom_call", output_to_operand_aliasing={{0}: (7, {})} | custom-call | tf_op jit(solution)/shard_map/second/pallas_call | solution.py:333
  102.9 13.3 %all_to_all.32.normed_ref = bf16[8,64,128]{2,1,0:T(8,128)(2,1)S(1)} all-to-all(bf16[8,64,128]{2,1,0:T(8,128)(2,1)S(1)} %get-tuple-element.30), channel_id=1, replica_groups=mesh['grp'=2,'tp'=16,'dp'=8] {'dp'}, dimensions={0} | all-to-all | bytes 262144 | tf_op jit(solution)/shard_map/all_to_all | solution.py:31
  116.2 0.0 copy-done.1
  116.2 0.3 branch.1
  116.6 14.0 %all_to_all.33 = f16[16,16,256]{2,1,0:T(8,128)(2,1)S(1)} all-to-all(f16[16,16,256]{2,1,0:T(8,128)(2,1)S(1)} %convert_element_type.26), channel_id=1, replica_groups=mesh['grp'=2,'tp'=16,'dp'=8] {'tp'}, dimensions={0} | all-to-all | bytes 262144 | tf_op jit(solution)/shard_map/all_to_all | solution.py:31
  130.6 0.6 final.1
  (13 shorter events, 0.2 us)
Async XLA Ops:
  0.6 51.8 %copy-start.7 = (s32[32]{0:T(128)S(1)}, s32[32]{0:T(128)}, u32[]{:S(2)}) copy-start(s32[32]{0:T(128)} %param.14) | copy-start | bytes 388
  0.6 55.2 %copy-start.6 = (f32[2,128]{1,0:T(2,128)S(1)}, f32[2,128]{1,0:T(2,128)}, u32[]{:S(2)}) copy-start(f32[2,128]{1,0:T(2,128)} %param.22) | copy-start | bytes 3076
  0.7 55.3 %copy-start.4 = (f32[2,128]{1,0:T(2,128)S(1)}, f32[2,128]{1,0:T(2,128)}, u32[]{:S(2)}) copy-start(f32[2,128]{1,0:T(2,128)} %head_ref.3) | copy-start | bytes 3076
  0.7 55.3 %copy-start.3 = (f32[2,128]{1,0:T(2,128)S(1)}, f32[2,128]{1,0:T(2,128)}, u32[]{:S(2)}) copy-start(f32[2,128]{1,0:T(2,128)} %bound_ref.3) | copy-start | bytes 3076
  2.1 33.0 %all-to-all-start = ((bf16[16,16,256]{2,1,0:T(8,128)(2,1)}), bf16[16,16,256]{2,1,0:T(8,128)(2,1)S(1)}, u32[]{:S(2)}, u32[]{:S(2)}) async-start(bf16[16,16,256]{2,1,0:T(8,128)(2,1)} %broadcast_in_dim.2), calls=%async_computation | async-start | bytes 262144 | tf_op jit(solution)/shard_map/all_to_all | solution.py:31
  25.8 0.7 copy-start.2
  36.1 19.8 %all-to-all-start.1 = ((f16[8,160,128]{2,1,0:T(8,128)(2,1)}), f16[8,160,128]{2,1,0:T(8,128)(2,1)S(1)}, u32[]{:S(2)}, u32[]{:S(2)}) async-start(f16[8,160,128]{2,1,0:T(8,128)(2,1)} %convert_element_type.21), calls=%async_computation.1 | async-start | bytes 655360 | tf_op jit(solution)/shard_map/all_to_all | solution.py:31
  40.6 15.2 %collective-permute-start.3 = (bf16[128,256]{1,0:T(8,128)(2,1)S(1)}, bf16[128,256]{1,0:T(8,128)(2,1)S(1)}, u32[]{:S(2)}, u32[]{:S(2)}) collective-permute-start(bf16[128,256]{1,0:T(8,128)(2,1)S(1)} %slice_bitcast_fusion.1.refs_0_), channel_id=1, source_target_pairs={{5,0},{4,1},{7,2},{6,3},{1,4},{0,5},{3,6},{2,7},{13,8},{12,9},{15,... | collective-permute-start | bytes 196616 | tf_op jit(solution)/shard_map/ppermute | solution.py:102
  44.9 16.1 %collective-permute-start.2 = (bf16[128,256]{1,0:T(8,128)(2,1)S(1)}, bf16[128,256]{1,0:T(8,128)(2,1)S(1)}, u32[]{:S(2)}, u32[]{:S(2)}) collective-permute-start(bf16[128,256]{1,0:T(8,128)(2,1)S(1)} %slice_bitcast_fusion.1.refs_0_), channel_id=1, source_target_pairs={{6,0},{3,1},{0,2},{5,3},{2,4},{7,5},{4,6},{1,7},{14,8},{11,9},{8,1... | collective-permute-start | bytes 196616 | tf_op jit(solution)/shard_map/ppermute | solution.py:102
  45.2 17.7 %collective-permute-start.1 = (bf16[128,256]{1,0:T(8,128)(2,1)S(1)}, bf16[128,256]{1,0:T(8,128)(2,1)S(1)}, u32[]{:S(2)}, u32[]{:S(2)}) collective-permute-start(bf16[128,256]{1,0:T(8,128)(2,1)S(1)} %slice_bitcast_fusion.1.refs_0_), channel_id=1, source_target_pairs={{7,0},{2,1},{1,2},{4,3},{3,4},{6,5},{5,6},{0,7},{15,8},{10,9},{9,1... | collective-permute-start | bytes 196616 | tf_op jit(solution)/shard_map/ppermute | solution.py:102
  47.8 47.7 %copy-start = (bf16[272,512]{1,0:T(8,128)(2,1)S(1)}, bf16[272,512]{1,0:T(8,128)(2,1)}, u32[]{:S(2)}) copy-start(bf16[272,512]{1,0:T(8,128)(2,1)} %pack.1.refs_0_) | copy-start | bytes 835588
  47.8 36.1 %collective-permute-start.6 = (bf16[272,512]{1,0:T(8,128)(2,1)}, bf16[272,512]{1,0:T(8,128)(2,1)S(1)}, u32[]{:S(2)}, u32[]{:S(2)}) collective-permute-start(bf16[272,512]{1,0:T(8,128)(2,1)} %pack.1.refs_0_), channel_id=1, source_target_pairs={{5,0},{4,1},{7,2},{6,3},{1,4},{0,5},{3,6},{2,7},{13,8},{12,9},{15,... | collective-permute-start | bytes 835592 | tf_op jit(solution)/shard_map/ppermute | solution.py:102
  52.2 31.7 %collective-permute-start.5 = (bf16[272,512]{1,0:T(8,128)(2,1)}, bf16[272,512]{1,0:T(8,128)(2,1)S(1)}, u32[]{:S(2)}, u32[]{:S(2)}) collective-permute-start(bf16[272,512]{1,0:T(8,128)(2,1)} %pack.1.refs_0_), channel_id=1, source_target_pairs={{6,0},{3,1},{0,2},{5,3},{2,4},{7,5},{4,6},{1,7},{14,8},{11,9},{8,1... | collective-permute-start | bytes 835592 | tf_op jit(solution)/shard_map/ppermute | solution.py:102
  55.8 28.0 %collective-permute-start.4 = (bf16[272,512]{1,0:T(8,128)(2,1)}, bf16[272,512]{1,0:T(8,128)(2,1)S(1)}, u32[]{:S(2)}, u32[]{:S(2)}) collective-permute-start(bf16[272,512]{1,0:T(8,128)(2,1)} %pack.1.refs_0_), channel_id=1, source_target_pairs={{7,0},{2,1},{1,2},{4,3},{3,4},{6,5},{5,6},{0,7},{15,8},{10,9},{9,1... | collective-permute-start | bytes 835592 | tf_op jit(solution)/shard_map/ppermute | solution.py:102
  56.0 40.0 %copy-start.5 = (f32[2,32,1,128,128]{4,3,2,1,0:T(8,128)S(1)}, f32[2,32,1,128,128]{4,3,2,1,0:T(8,128)}, u32[]{:S(2)}) copy-start(f32[2,32,1,128,128]{4,3,2,1,0:T(8,128)} %state_ref.1) | copy-start | bytes 12582916
  61.0 4.3 %collective-permute-start = (bf16[64,128]{1,0:T(8,128)(2,1)S(1)}, bf16[64,128]{1,0:T(8,128)(2,1)S(1)}, u32[]{:S(2)}, u32[]{:S(2)}) collective-permute-start(bf16[64,128]{1,0:T(8,128)(2,1)S(1)} %get-tuple-element.23), channel_id=1, source_target_pairs={{0,1},{1,0},{2,3},{3,2},{4,5},{5,4},{6,7},{7,6},{8,9},{9,8},{10,11... | collective-permute-start | bytes 49160 | tf_op jit(solution)/shard_map/ppermute | solution.py:107
  95.9 4.3 %collective-permute-start.7 = (f32[32,640]{1,0:T(8,128)S(1)}, f32[32,640]{1,0:T(8,128)S(1)}, u32[]{:S(2)}, u32[]{:S(2)}) collective-permute-start(f32[32,640]{1,0:T(8,128)S(1)} %get-tuple-element.26), channel_id=1, source_target_pairs={{0,1},{1,0},{2,3},{3,2},{4,5},{5,4},{6,7},{7,6},{8,9},{9,8},{10,11... | collective-permute-start | bytes 245768 | tf_op jit(solution)/shard_map/ppermute | solution.py:107
  96.2 20.0 %copy-start.1 = (bf16[2,128,256]{2,1,0:T(8,128)(2,1)S(1)}, bf16[2,128,256]{2,1,0:T(8,128)(2,1)}, u32[]{:S(2)}) copy-start(bf16[2,128,256]{2,1,0:T(8,128)(2,1)} %w_ref.1) | copy-start | bytes 393220

commit v3 on v2

--- a/solution.py
+++ b/solution.py
@@ -14,8 +14,7 @@
 PAD = 16
 LANES = 32
 SHARE_AT = 16
-STEP = 4
-AHEAD = 3
+STEP = 8
 PARAMS = pltpu.CompilerParams(vmem_limit_bytes=16 << 20)
 SECOND_PARAMS = pltpu.CompilerParams(vmem_limit_bytes=50 << 20)
 WIDE_PARAMS = pltpu.CompilerParams(vmem_limit_bytes=51 << 20)
@@ -157,6 +156,25 @@
     )(whole, gain, *weights)
 
 
+def load_kernel(ready_ref, state_ref, out_ref, sem):
+    copy = pltpu.make_async_copy(state_ref.at[1, :, 0], out_ref, sem)
+    copy.start()
+    copy.wait()
+
+
+def load(ready, state):
+    _, count, _, size, _ = state.shape
+    return pl.pallas_call(
+        load_kernel,
+        in_specs=[VMEM, HBM],
+        out_specs=VMEM,
+        out_shape=jax.ShapeDtypeStruct((count, size, size), jnp.float32),
+        scratch_shapes=[pltpu.SemaphoreType.DMA],
+        compiler_params=WIDE_PARAMS,
+        name="load",
+    )(ready, state)
+
+
 def recur(block, made, shift_ref, bound_ref, head_ref, prior_ref, new_ref, loads, stores):
     query, forget_in, value, gate = made
     lower = jax.nn.sigmoid(bound_ref[block : block + 1, :])
@@ -169,8 +187,6 @@
     for n in range(value.shape[0]):
         if loads and n % STEP == 0:
             loads[n // STEP].wait()
-            if n // STEP + AHEAD < len(loads):
-                loads[n // STEP + AHEAD].start()
         at = slice(n, n + 1)
         updated = forget[:, at] * prior_ref[n] + key[:, at] * value[at, :]
         new_ref[n] = updated
@@ -189,7 +205,7 @@
         rows = pl.ds(n * STEP, STEP)
         loads.append(pltpu.make_async_copy(state_ref.at[0, rows, 0], prior_s.at[rows], in_sems.at[n]))
         stores.append(pltpu.make_async_copy(new_s.at[rows], new_ref.at[0, rows, 0], out_sems.at[n]))
-    for load in loads[:AHEAD]:
+    for load in loads:
         load.start()
     owners, _, size = parts_ref.shape
     count = shift_ref.shape[1]
@@ -397,7 +413,8 @@
     message = project(whole, gain, firsts, dp).astype(jnp.float16)
     parts = exchange(message, "dp").astype(jnp.float32)
     target, own, sent = first(parts, shift, bound_logit, head_gain, tokens.shape[1] // tp, state)
-    held = near(pack(1, norm_gain, weights), "dp")
+    packed = pack(1, norm_gain, weights)
+    held = near(packed, "dp")
     came = swap(sent, "dp")
     sums = pair_parts(own, came, back)
     parts = exchange_products(sums, "tp")
@@ -408,7 +425,7 @@
         name="next",
     )(parts)
     joined = exchange(after(copies, held[1:]), "tp")
-    prior = after(state, joined)[1, :, 0]
+    prior = load(after(gain, joined), state)
     own, sent, kept = again(joined, held, dp)
     came = swap(sent, "dp")
     target, normed = second(own, came, shift, bound_logit, head_gain, kept, prior, target)

time: 132 us -> 131 us (level)
  waiting for transfers between devices: 17.3 us -> 14.6 us
    ppermute x2, waiting for transfers between devices: 6.3 us -> 3.65 us  [swap(): lax.ppermute(x, axis, [(n, n ^ 1) for n in range(lax.axis_size(axis))])]
    pallas_call x0 -> x1, Pallas kernels: none -> 1.6 us  [load(): pl.pallas_call(load_kernel, in_specs=[VMEM, HBM], out_specs=VMEM, out_sha...]
where the time goes in v3:
time: 131 us; the launch traced here: 130 us
  blocking collectives  58.4 us (45%)
  starting transfers between devices  38.9 us (30%)
  waiting for transfers between devices  14.6 us (11%)
  Pallas kernels  13.7 us (10%)
  local copies, waits for them, and re-layouts  2.93 us (2%)
    all_to_all x4, blocking collectives, exchange(): return lax.all_to_all(x, axis, split_axis=0, concat_axis=0, tiled=True)  58.4 us
    all_to_all x2, starting transfers between devices, exchange(): return lax.all_to_all(x, axis, split_axis=0, concat_axis=0, tiled=True)  27.4 us
    ppermute x6, starting transfers between devices, near(): held.append(lax.ppermute(shard, axis, pairs))  9.46 us
    all_to_all x2, waiting for transfers between devices, exchange(): return lax.all_to_all(x, axis, split_axis=0, concat_axis=0, tiled=True)  7.6 us
    pallas_call x1, Pallas kernels, first(): pl.pallas_call(functools.partial(first_kernel, share), in_specs=[VMEM] *...  4.04 us
    ppermute x2, waiting for transfers between devices, swap(): lax.ppermute(x, axis, [(n, n ^ 1) for n in range(lax.axis_size(axis))])  3.65 us
    ppermute x6, waiting for transfers between devices, near(): held.append(lax.ppermute(shard, axis, pairs))  3.39 us
    pallas_call x1, Pallas kernels, second(): pl.pallas_call(second_kernel, in_specs=[VMEM] * 7 + [HBM], out_specs=[HBM...  2.76 us
  transfers between devices with their start and end apart: 10, of which 4 were waited for; matrix products, arithmetic and copies ran while one was open for 1% of the time, Pallas kernels for 7%

profile of v3, /device:TPU:513, one launch (start us, length us, event | category | flops | bytes accessed | tf_op | source)
XLA Modules:
  0.0 130.4 jit_solution(11863508090976518036)
XLA Ops:
  0.6 0.0 copy-start.6
  0.6 0.0 copy-start.5
  0.7 0.0 copy-start.4
  0.7 0.0 copy-start.3
  0.7 1.4 %broadcast_in_dim.2 = bf16[16,16,256]{2,1,0:T(8,128)(2,1)} broadcast(bf16[16,256]{1,0:T(8,128)(2,1)} %param.12), dimensions={1,2} | broadcast | bytes 139264 | tf_op jit(solution)/shard_map/broadcast_in_dim | solution.py:406
  2.1 23.7 %all-to-all-start = ((bf16[16,16,256]{2,1,0:T(8,128)(2,1)}), bf16[16,16,256]{2,1,0:T(8,128)(2,1)S(1)}, u32[]{:S(2)}, u32[]{:S(2)}) async-start(bf16[16,16,256]{2,1,0:T(8,128)(2,1)} %broadcast_in_dim.2), calls=%async_computation | async-start | bytes 262144 | tf_op jit(solution)/shard_map/all_to_all | solution.py:30
  25.8 0.7 copy-done.2
  26.5 1.0 prep.1
  27.4 7.6 %all-to-all-done.x_ref = bf16[16,16,256]{2,1,0:T(8,128)(2,1)S(1)} async-done(((bf16[16,16,256]{2,1,0:T(8,128)(2,1)}), bf16[16,16,256]{2,1,0:T(8,128)(2,1)S(1)}, u32[]{:S(2)}, u32[]{:S(2)}) %all-to-all-start) | async-done | bytes 131104 | tf_op jit(solution)/shard_map/all_to_all | solution.py:30
  35.0 0.3 project.1
  35.4 0.8 convert_element_type.21
  36.1 3.6 %all-to-all-start.1 = ((f16[8,160,128]{2,1,0:T(8,128)(2,1)}), f16[8,160,128]{2,1,0:T(8,128)(2,1)S(1)}, u32[]{:S(2)}, u32[]{:S(2)}) async-start(f16[8,160,128]{2,1,0:T(8,128)(2,1)} %convert_element_type.21), calls=%async_computation.1 | async-start | bytes 655360 | tf_op jit(solution)/shard_map/all_to_all | solution.py:30
  39.8 0.8 slice_bitcast_fusion.refs_0_
  40.6 4.3 %collective-permute-start.3 = (bf16[128,256]{1,0:T(8,128)(2,1)S(1)}, bf16[128,256]{1,0:T(8,128)(2,1)S(1)}, u32[]{:S(2)}, u32[]{:S(2)}) collective-permute-start(bf16[128,256]{1,0:T(8,128)(2,1)S(1)} %slice_bitcast_fusion.refs_0_), channel_id=1, source_target_pairs={{5,0},{4,1},{7,2},{6,3},{1,4},{0,5},{3,6},{2,7},{13,8},{12,9},{15,... | collective-permute-start | bytes 196616 | tf_op jit(solution)/shard_map/ppermute | solution.py:101
  44.9 0.3 collective-permute-start.2
  45.2 0.2 collective-permute-start.1
  45.4 2.3 %pack.1.refs_0_ = bf16[272,512]{1,0:T(8,128)(2,1)} custom-call(bf16[2,256]{1,0:T(2,128)(2,1)} %gain_ref.3, bf16[2,256,128]{2,1,0:T(8,128)(2,1)} %wq_ref.1, bf16[2,256,128]{2,1,0:T(8,128)(2,1)} %wf_ref.1, bf16[2,256,128]{2,1,0:T(8,128)(2,1)} %wi_ref.1, bf16[2,256,128]{2,1,0:T(8,128)(2,1)} %wg_ref.1), custom_call_target="tpu_custom_call" | custom-call | tf_op jit(solution)/shard_map/pack/pallas_call | solution.py:54
  47.8 0.0 copy-start
  47.8 4.4 %collective-permute-start.6 = (bf16[272,512]{1,0:T(8,128)(2,1)}, bf16[272,512]{1,0:T(8,128)(2,1)S(1)}, u32[]{:S(2)}, u32[]{:S(2)}) collective-permute-start(bf16[272,512]{1,0:T(8,128)(2,1)} %pack.1.refs_0_), channel_id=1, source_target_pairs={{5,0},{4,1},{7,2},{6,3},{1,4},{0,5},{3,6},{2,7},{13,8},{12,9},{15,... | collective-permute-start | bytes 835592 | tf_op jit(solution)/shard_map/ppermute | solution.py:101
  52.1 0.3 collective-permute-start.5
  52.5 0.0 copy-done.6
  52.5 3.4 %collective-permute-done.3.refs_3_ = bf16[128,256]{1,0:T(8,128)(2,1)S(1)} collective-permute-done((bf16[128,256]{1,0:T(8,128)(2,1)S(1)}, bf16[128,256]{1,0:T(8,128)(2,1)S(1)}, u32[]{:S(2)}, u32[]{:S(2)}) %collective-permute-start.3) | collective-permute-done | bytes 65568 | tf_op jit(solution)/shard_map/ppermute | solution.py:101
  55.8 0.0 collective-permute-start.4
  55.9 0.0 copy-done.5
  55.9 0.1 broadcast_multiply_fusion.shift_ref
  55.9 0.0 all-to-all-done.1
  56.0 4.0 %first.1 = (f32[2,32,1,128,128]{4,3,2,1,0:T(8,128)}, bf16[64,128]{1,0:T(8,128)(2,1)S(1)}, bf16[64,128]{1,0:T(8,128)(2,1)S(1)}) custom-call(f32[8,160,128]{2,1,0:T(8,128)S(1)} %convert_element_type.22.parts_ref, f32[2,32,128]{2,1,0:T(8,128)S(1)} %broadcast_multiply_fusion.shift_ref, f32[2,128]{1,0:T(2,128)S(1)} %copy-done.3, f32[2,128]{1,0:T(2,128)S(1)} %copy-done.4, ...), custom_call_target="tpu_custom_call" | custom-call | tf_op jit(solution)/shard_map/first/pallas_call | solution.py:270
  60.0 0.0 collective-permute-done.2.refs_2_
  60.1 2.0 %collective-permute-start = (bf16[64,128]{1,0:T(8,128)(2,1)S(1)}, bf16[64,128]{1,0:T(8,128)(2,1)S(1)}, u32[]{:S(2)}, u32[]{:S(2)}) collective-permute-start(bf16[64,128]{1,0:T(8,128)(2,1)S(1)} %get-tuple-element.23), channel_id=1, source_target_pairs={{0,1},{1,0},{2,3},{3,2},{4,5},{5,4},{6,7},{7,6},{8,9},{9,8},{10,11... | collective-permute-start | bytes 49160 | tf_op jit(solution)/shard_map/ppermute | solution.py:106
  62.0 0.0 collective-permute-done.1.refs_1_
  62.0 1.2 collective-permute-done.came_ref
  63.2 0.3 pair.1
  63.5 19.4 %all_to_all.30 = f16[16,32,128]{2,1,0:T(8,128)(2,1)S(1)} all-to-all(f16[16,32,128]{2,1,0:T(8,128)(2,1)S(1)} %convert_element_type.24), channel_id=1, replica_groups=mesh['grp'=2,'tp'=16,'dp'=8] {'tp'}, dimensions={0} | all-to-all | bytes 262144 | tf_op jit(solution)/shard_map/all_to_all | solution.py:30
  83.0 0.0 collective-permute-done.6.refs_3_
  83.0 0.0 collective-permute-done.5.refs_2_
  83.0 0.0 collective-permute-done.4.refs_1_
  83.0 11.6 %all_to_all.31.x_ref = bf16[16,32,128]{2,1,0:T(8,128)(2,1)S(1)} all-to-all(bf16[16,32,128]{2,1,0:T(8,128)(2,1)S(1)} %next.1), channel_id=1, replica_groups=mesh['grp'=2,'tp'=16,'dp'=8] {'tp'}, dimensions={0} | all-to-all | bytes 262144 | tf_op jit(solution)/shard_map/all_to_all | solution.py:30
  94.6 0.4 again.1
  95.0 0.1 collective-permute-start.7
  95.1 1.6 %load.1.prior_ref = f32[32,128,128]{2,1,0:T(8,128)S(1)} custom-call(f32[1,256]{1,0:T(1,128)S(1)} %get-tuple-element.28.gain_ref.ready_ref, f32[2,32,1,128,128]{4,3,2,1,0:T(8,128)} %state_ref.3), custom_call_target="tpu_custom_call" | custom-call | tf_op jit(solution)/shard_map/load/pallas_call | solution.py:167
  96.7 0.0 copy-start.1
  96.8 2.5 %collective-permute-done.7.came_ref = f32[32,640]{1,0:T(8,128)S(1)} collective-permute-done((f32[32,640]{1,0:T(8,128)S(1)}, f32[32,640]{1,0:T(8,128)S(1)}, u32[]{:S(2)}, u32[]{:S(2)}) %collective-permute-start.7) | collective-permute-done | bytes 81952 | tf_op jit(solution)/shard_map/ppermute | solution.py:106
  99.2 2.8 %second.1 = (f32[2,32,1,128,128]{4,3,2,1,0:T(8,128)}, bf16[8,64,128]{2,1,0:T(8,128)(2,1)S(1)}) custom-call(f32[32,640]{1,0:T(8,128)S(1)} %get-tuple-element.25.own_ref, f32[32,640]{1,0:T(8,128)S(1)} %collective-permute-done.7.came_ref, f32[2,32,128]{2,1,0:T(8,128)S(1)} %broadcast_multiply_fusion.shift_ref, ...), custom_call_target="tpu_custom_call", output_to_operand_aliasing={{0}: (7, {})} | custom-call | tf_op jit(solution)/shard_map/second/pallas_call | solution.py:349
  102.0 13.4 %all_to_all.32.normed_ref = bf16[8,64,128]{2,1,0:T(8,128)(2,1)S(1)} all-to-all(bf16[8,64,128]{2,1,0:T(8,128)(2,1)S(1)} %get-tuple-element.30), channel_id=1, replica_groups=mesh['grp'=2,'tp'=16,'dp'=8] {'dp'}, dimensions={0} | all-to-all | bytes 262144 | tf_op jit(solution)/shard_map/all_to_all | solution.py:30
  115.4 0.0 copy-done.1
  115.4 0.3 branch.1
  115.7 14.0 %all_to_all.33 = f16[16,16,256]{2,1,0:T(8,128)(2,1)S(1)} all-to-all(f16[16,16,256]{2,1,0:T(8,128)(2,1)S(1)} %convert_element_type.26), channel_id=1, replica_groups=mesh['grp'=2,'tp'=16,'dp'=8] {'tp'}, dimensions={0} | all-to-all | bytes 262144 | tf_op jit(solution)/shard_map/all_to_all | solution.py:30
  129.8 0.6 final.1
  (11 shorter events, 0.2 us)
Async XLA Ops:
  0.6 51.8 %copy-start.6 = (s32[32]{0:T(128)S(1)}, s32[32]{0:T(128)}, u32[]{:S(2)}) copy-start(s32[32]{0:T(128)} %param.14) | copy-start | bytes 388
  0.6 55.2 %copy-start.5 = (f32[2,128]{1,0:T(2,128)S(1)}, f32[2,128]{1,0:T(2,128)}, u32[]{:S(2)}) copy-start(f32[2,128]{1,0:T(2,128)} %param.22) | copy-start | bytes 3076
  0.7 55.3 %copy-start.4 = (f32[2,128]{1,0:T(2,128)S(1)}, f32[2,128]{1,0:T(2,128)}, u32[]{:S(2)}) copy-start(f32[2,128]{1,0:T(2,128)} %head_ref.3) | copy-start | bytes 3076
  0.7 55.3 %copy-start.3 = (f32[2,128]{1,0:T(2,128)S(1)}, f32[2,128]{1,0:T(2,128)}, u32[]{:S(2)}) copy-start(f32[2,128]{1,0:T(2,128)} %bound_ref.3) | copy-start | bytes 3076
  2.1 33.0 %all-to-all-start = ((bf16[16,16,256]{2,1,0:T(8,128)(2,1)}), bf16[16,16,256]{2,1,0:T(8,128)(2,1)S(1)}, u32[]{:S(2)}, u32[]{:S(2)}) async-start(bf16[16,16,256]{2,1,0:T(8,128)(2,1)} %broadcast_in_dim.2), calls=%async_computation | async-start | bytes 262144 | tf_op jit(solution)/shard_map/all_to_all | solution.py:30
  25.8 0.7 copy-start.2
  36.1 19.8 %all-to-all-start.1 = ((f16[8,160,128]{2,1,0:T(8,128)(2,1)}), f16[8,160,128]{2,1,0:T(8,128)(2,1)S(1)}, u32[]{:S(2)}, u32[]{:S(2)}) async-start(f16[8,160,128]{2,1,0:T(8,128)(2,1)} %convert_element_type.21), calls=%async_computation.1 | async-start | bytes 655360 | tf_op jit(solution)/shard_map/all_to_all | solution.py:30
  40.6 15.2 %collective-permute-start.3 = (bf16[128,256]{1,0:T(8,128)(2,1)S(1)}, bf16[128,256]{1,0:T(8,128)(2,1)S(1)}, u32[]{:S(2)}, u32[]{:S(2)}) collective-permute-start(bf16[128,256]{1,0:T(8,128)(2,1)S(1)} %slice_bitcast_fusion.refs_0_), channel_id=1, source_target_pairs={{5,0},{4,1},{7,2},{6,3},{1,4},{0,5},{3,6},{2,7},{13,8},{12,9},{15,... | collective-permute-start | bytes 196616 | tf_op jit(solution)/shard_map/ppermute | solution.py:101
  44.9 15.2 %collective-permute-start.2 = (bf16[128,256]{1,0:T(8,128)(2,1)S(1)}, bf16[128,256]{1,0:T(8,128)(2,1)S(1)}, u32[]{:S(2)}, u32[]{:S(2)}) collective-permute-start(bf16[128,256]{1,0:T(8,128)(2,1)S(1)} %slice_bitcast_fusion.refs_0_), channel_id=1, source_target_pairs={{6,0},{3,1},{0,2},{5,3},{2,4},{7,5},{4,6},{1,7},{14,8},{11,9},{8,1... | collective-permute-start | bytes 196616 | tf_op jit(solution)/shard_map/ppermute | solution.py:101
  45.2 16.8 %collective-permute-start.1 = (bf16[128,256]{1,0:T(8,128)(2,1)S(1)}, bf16[128,256]{1,0:T(8,128)(2,1)S(1)}, u32[]{:S(2)}, u32[]{:S(2)}) collective-permute-start(bf16[128,256]{1,0:T(8,128)(2,1)S(1)} %slice_bitcast_fusion.refs_0_), channel_id=1, source_target_pairs={{7,0},{2,1},{1,2},{4,3},{3,4},{6,5},{5,6},{0,7},{15,8},{10,9},{9,1... | collective-permute-start | bytes 196616 | tf_op jit(solution)/shard_map/ppermute | solution.py:101
  47.8 46.8 %copy-start = (bf16[272,512]{1,0:T(8,128)(2,1)S(1)}, bf16[272,512]{1,0:T(8,128)(2,1)}, u32[]{:S(2)}) copy-start(bf16[272,512]{1,0:T(8,128)(2,1)} %pack.1.refs_0_) | copy-start | bytes 835588
  47.8 35.2 %collective-permute-start.6 = (bf16[272,512]{1,0:T(8,128)(2,1)}, bf16[272,512]{1,0:T(8,128)(2,1)S(1)}, u32[]{:S(2)}, u32[]{:S(2)}) collective-permute-start(bf16[272,512]{1,0:T(8,128)(2,1)} %pack.1.refs_0_), channel_id=1, source_target_pairs={{5,0},{4,1},{7,2},{6,3},{1,4},{0,5},{3,6},{2,7},{13,8},{12,9},{15,... | collective-permute-start | bytes 835592 | tf_op jit(solution)/shard_map/ppermute | solution.py:101
  52.1 30.8 %collective-permute-start.5 = (bf16[272,512]{1,0:T(8,128)(2,1)}, bf16[272,512]{1,0:T(8,128)(2,1)S(1)}, u32[]{:S(2)}, u32[]{:S(2)}) collective-permute-start(bf16[272,512]{1,0:T(8,128)(2,1)} %pack.1.refs_0_), channel_id=1, source_target_pairs={{6,0},{3,1},{0,2},{5,3},{2,4},{7,5},{4,6},{1,7},{14,8},{11,9},{8,1... | collective-permute-start | bytes 835592 | tf_op jit(solution)/shard_map/ppermute | solution.py:101
  55.8 27.1 %collective-permute-start.4 = (bf16[272,512]{1,0:T(8,128)(2,1)}, bf16[272,512]{1,0:T(8,128)(2,1)S(1)}, u32[]{:S(2)}, u32[]{:S(2)}) collective-permute-start(bf16[272,512]{1,0:T(8,128)(2,1)} %pack.1.refs_0_), channel_id=1, source_target_pairs={{7,0},{2,1},{1,2},{4,3},{3,4},{6,5},{5,6},{0,7},{15,8},{10,9},{9,1... | collective-permute-start | bytes 835592 | tf_op jit(solution)/shard_map/ppermute | solution.py:101
  60.1 3.1 %collective-permute-start = (bf16[64,128]{1,0:T(8,128)(2,1)S(1)}, bf16[64,128]{1,0:T(8,128)(2,1)S(1)}, u32[]{:S(2)}, u32[]{:S(2)}) collective-permute-start(bf16[64,128]{1,0:T(8,128)(2,1)S(1)} %get-tuple-element.23), channel_id=1, source_target_pairs={{0,1},{1,0},{2,3},{3,2},{4,5},{5,4},{6,7},{7,6},{8,9},{9,8},{10,11... | collective-permute-start | bytes 49160 | tf_op jit(solution)/shard_map/ppermute | solution.py:106
  95.0 4.3 %collective-permute-start.7 = (f32[32,640]{1,0:T(8,128)S(1)}, f32[32,640]{1,0:T(8,128)S(1)}, u32[]{:S(2)}, u32[]{:S(2)}) collective-permute-start(f32[32,640]{1,0:T(8,128)S(1)} %get-tuple-element.26), channel_id=1, source_target_pairs={{0,1},{1,0},{2,3},{3,2},{4,5},{5,4},{6,7},{7,6},{8,9},{9,8},{10,11... | collective-permute-start | bytes 245768 | tf_op jit(solution)/shard_map/ppermute | solution.py:106
  96.7 18.6 %copy-start.1 = (bf16[2,128,256]{2,1,0:T(8,128)(2,1)S(1)}, bf16[2,128,256]{2,1,0:T(8,128)(2,1)}, u32[]{:S(2)}) copy-start(bf16[2,128,256]{2,1,0:T(8,128)(2,1)} %w_ref.1) | copy-start | bytes 393220

commit v4 on v3

--- a/solution.py
+++ b/solution.py
@@ -121,6 +121,14 @@
 def code(total):
     root = jnp.sqrt(jnp.abs(total)) * 2.0**6
     return jnp.where(total < 0.0, -root, root)
+
+
+def scaled(squares, bits):
+    power = jnp.ceil(0.5 * jnp.log2(jnp.maximum(squares, FLOOR)))
+    down = jnp.exp2(-power)
+    mantissa = squares * down * down
+    high = mantissa.astype(jnp.bfloat16).astype(jnp.float32)
+    return down * 2.0**bits, (power - bits, high, mantissa - high)
 
 
 def project_kernel(share, x_ref, gain_ref, wq_ref, wf_ref, wi_ref, wg_ref, out_ref):
@@ -290,7 +298,8 @@
 
 def again_kernel(share, x_ref, *refs):
     shards, (own_ref, sent_ref, kept_ref) = refs[:-3], refs[-3:]
-    owners, count, size = kept_ref.shape
+    owners, packed, size = kept_ref.shape
+    count = x_ref.shape[1]
     rows = shards[0].shape[0] - PAD
     parts = rows // size
     blocks = len(shards) * parts
@@ -309,11 +318,18 @@
         gained = (wide * shard[rows : rows + 1, :rows].astype(jnp.float32)).astype(jnp.bfloat16)
         made += jnp.dot(gained, shard[:rows, :], preferred_element_type=jnp.float32)
         kept = [jnp.dot(halves[half], choose[half], preferred_element_type=jnp.float32) for half in range(2)]
-        kept_ref[near_chunk(n, owners)] = (kept[0] + kept[1]).astype(kept_ref.dtype)
-    for half, out_ref in enumerate((own_ref, sent_ref)):
-        row = slice(half * count, (half + 1) * count)
-        out_ref[:, : made.shape[1]] = made[row]
-        out_ref[:, made.shape[1] :] = jnp.broadcast_to(squares[row], (count, size))
+        kept = kept[0] + kept[1]
+        block = kept[:packed]
+        for group in range(1, count // packed):
+            block += pltpu.roll(kept[group * packed : (group + 1) * packed], group * LANES, 1)
+        kept_ref[near_chunk(n, owners)] = block.astype(kept_ref.dtype)
+    own_ref[:, : made.shape[1]] = made[:count]
+    own_ref[:, made.shape[1] :] = jnp.broadcast_to(squares[:count], (count, size))
+    factor, columns = scaled(squares[count:], 12)
+    sent_ref[:, : made.shape[1]] = factor * made[count:]
+    lane = lax.broadcasted_iota(jnp.int32, (count, size), 1)
+    table = jnp.where(lane == 0, columns[0], jnp.where(lane == 1, columns[1], jnp.where(lane == 2, columns[2], 0.0)))
+    sent_ref[:, made.shape[1] :] = table
 
 
 def again(x, shards, owners):
@@ -322,21 +338,26 @@
     sums = jax.ShapeDtypeStruct((count, shards[0].shape[1] + size), jnp.float32)
     return pl.pallas_call(
         functools.partial(again_kernel, rows // tp),
-        out_shape=[sums, sums, jax.ShapeDtypeStruct((owners, count, size), jnp.bfloat16)],
+        out_shape=[sums, sums, jax.ShapeDtypeStruct((owners, count * LANES // size, size), jnp.bfloat16)],
         compiler_params=PARAMS,
         name="again",
     )(x, *shards)
 
 
 def second_kernel(own_ref, came_ref, shift_ref, bound_ref, head_ref, kept_ref, prior_ref, _, new_ref, out_ref, new_s, sems):
-    owners, count, size = kept_ref.shape
+    owners, _, size = kept_ref.shape
+    count = shift_ref.shape[1]
     stores = []
     for n in range(count // STEP):
         rows = pl.ds(n * STEP, STEP)
         stores.append(pltpu.make_async_copy(new_s.at[rows], new_ref.at[1, rows, 0], sems.at[n]))
-    total = own_ref[...] + came_ref[...]
-    scale = lax.rsqrt(total[:, 4 * size : 4 * size + 1] / D + epsilon)
-    made = [scale * total[:, n * size : (n + 1) * size] for n in range(4)]
+    table = came_ref[:, 4 * size :]
+    up = jnp.exp2(table[:, 0:1])
+    norm = up * 2.0**12
+    squares = own_ref[:, 4 * size : 4 * size + 1] + (table[:, 1:2] + table[:, 2:3]) * norm * norm
+    scale = lax.rsqrt(squares / D + epsilon)
+    lanes = [slice(n * size, (n + 1) * size) for n in range(4)]
+    made = [scale * (own_ref[:, lane] + up * came_ref[:, lane]) for lane in lanes]
     out_ref[:, count:, :] = kept_ref[...]
     normed = recur(1, made, shift_ref, bound_ref, head_ref, prior_ref, new_s, (), stores)
     out_ref[:, :count, :] = jnp.broadcast_to(normed, (owners, count, size))
@@ -345,14 +366,15 @@
 
 
 def second(own, came, shift, bound, head, kept, prior, target):
-    owners, count, size = kept.shape
+    owners, packed, size = kept.shape
+    count = prior.shape[0]
     return pl.pallas_call(
         second_kernel,
         in_specs=[VMEM] * 7 + [HBM],
         out_specs=[HBM, VMEM],
         out_shape=[
             jax.ShapeDtypeStruct(target.shape, jnp.float32),
-            jax.ShapeDtypeStruct((owners, 2 * count, size), jnp.bfloat16),
+            jax.ShapeDtypeStruct((owners, count + packed, size), jnp.bfloat16),
         ],
         scratch_shapes=[pltpu.VMEM(prior.shape, jnp.float32), pltpu.SemaphoreType.DMA((count // STEP,))],
         input_output_aliases={7: 0},
@@ -361,24 +383,30 @@
     )(own, came, shift, bound, head, kept, prior, target)
 
 
-def branch_kernel(share, normed_ref, w_ref, out_ref):
-    owners, count, size = normed_ref.shape[0], normed_ref.shape[1] // 2, normed_ref.shape[2]
+def branch_kernel(share, count, normed_ref, w_ref, out_ref):
+    owners, both, size = normed_ref.shape
+    packed = both - count
     normed = normed_ref[:, :count, :].reshape(-1, size)
     weight = w_ref[1]
     total = jnp.dot(normed, weight, preferred_element_type=jnp.float32)
     at = lax.axis_index("tp") * share
-    mine, other = (selection(size, weight.shape[1], half * share, at, share) for half in range(2))
-    flipped = jnp.concatenate([normed_ref[n ^ 1, count:, :] for n in range(owners)], axis=0)
-    total += jnp.dot(normed_ref[:, count:, :].reshape(-1, size), mine, preferred_element_type=jnp.float32)
-    total += jnp.dot(flipped, other, preferred_element_type=jnp.float32)
-    out_ref[...] = code(total).reshape(out_ref.shape)
-
-
-def branch_parts(normed, weight, owners):
-    rows = normed.shape[0] * normed.shape[1] // 2 // owners
-    return pl.pallas_call(
-        functools.partial(branch_kernel, weight.shape[2] // owners),
-        out_shape=jax.ShapeDtypeStruct((owners, rows, weight.shape[2]), jnp.float32),
+    held = [normed_ref[:, count:, :].reshape(-1, size)]
+    held.append(jnp.concatenate([normed_ref[n ^ 1, count:, :] for n in range(owners)], axis=0))
+    groups = []
+    for group in range(count // packed):
+        kept = 0.0
+        for half in range(2):
+            place = selection(size, weight.shape[1], group * LANES + half * share, at, share)
+            kept += jnp.dot(held[half], place, preferred_element_type=jnp.float32)
+        groups.append(kept)
+    rows = [groups[g][n * packed : (n + 1) * packed] for n in range(owners) for g in range(len(groups))]
+    out_ref[...] = code(total + jnp.concatenate(rows, axis=0)).reshape(out_ref.shape)
+
+
+def branch_parts(normed, weight, owners, count):
+    return pl.pallas_call(
+        functools.partial(branch_kernel, weight.shape[2] // owners, count),
+        out_shape=jax.ShapeDtypeStruct((owners, normed.shape[0] * count // owners, weight.shape[2]), jnp.float32),
         compiler_params=PARAMS,
         name="branch",
     )(normed, weight)
@@ -427,9 +455,9 @@
     joined = exchange(after(copies, held[1:]), "tp")
     prior = load(after(gain, joined), state)
     own, sent, kept = again(joined, held, dp)
-    came = swap(sent, "dp")
+    came = swap(sent.astype(jnp.float16), "dp").astype(jnp.float32)
     target, normed = second(own, came, shift, bound_logit, head_gain, kept, prior, target)
-    parts = exchange_products(branch_parts(exchange(normed, "dp"), w_out, tp), "tp")
+    parts = exchange_products(branch_parts(exchange(normed, "dp"), w_out, tp, lengths.shape[0]), "tp")
     result = pl.pallas_call(
         final_kernel,
         out_shape=jax.ShapeDtypeStruct(tokens.shape, jnp.float32),

time: 131 us -> 130 us (level)
  no operation moved by 1% of the time
where the time goes in v4:
time: 130 us; the launch traced here: 129 us
  blocking collectives  57.7 us (44%)
  starting transfers between devices  38.9 us (30%)
  Pallas kernels  14 us (11%)
  waiting for transfers between devices  13.8 us (11%)
  local copies, waits for them, and re-layouts  2.93 us (2%)
    all_to_all x4, blocking collectives, exchange(): return lax.all_to_all(x, axis, split_axis=0, concat_axis=0, tiled=True)  57.7 us
    all_to_all x2, starting transfers between devices, exchange(): return lax.all_to_all(x, axis, split_axis=0, concat_axis=0, tiled=True)  27.4 us
    ppermute x6, starting transfers between devices, near(): held.append(lax.ppermute(shard, axis, pairs))  9.46 us
    all_to_all x2, waiting for transfers between devices, exchange(): return lax.all_to_all(x, axis, split_axis=0, concat_axis=0, tiled=True)  7.6 us
    pallas_call x1, Pallas kernels, first(): pl.pallas_call(functools.partial(first_kernel, share), in_specs=[VMEM] *...  4.04 us
    ppermute x6, waiting for transfers between devices, near(): held.append(lax.ppermute(shard, axis, pairs))  3.39 us
    pallas_call x1, Pallas kernels, second(): pl.pallas_call(second_kernel, in_specs=[VMEM] * 7 + [HBM], out_specs=[HBM...  2.93 us
    ppermute x2, waiting for transfers between devices, swap(): lax.ppermute(x, axis, [(n, n ^ 1) for n in range(lax.axis_size(axis))])  2.78 us
  transfers between devices with their start and end apart: 10, of which 4 were waited for; matrix products, arithmetic and copies ran while one was open for 1% of the time, Pallas kernels for 7%

profile of v4, /device:TPU:513, one launch (start us, length us, event | category | flops | bytes accessed | tf_op | source)
XLA Modules:
  0.0 129.2 jit_solution(4080420113332595487)
XLA Ops:
  0.6 0.0 copy-start.6
  0.6 0.0 copy-start.5
  0.7 0.0 copy-start.4
  0.7 0.0 copy-start.3
  0.7 1.4 %broadcast_in_dim.2 = bf16[16,16,256]{2,1,0:T(8,128)(2,1)} broadcast(bf16[16,256]{1,0:T(8,128)(2,1)} %param.12), dimensions={1,2} | broadcast | bytes 139264 | tf_op jit(solution)/shard_map/broadcast_in_dim | solution.py:434
  2.1 23.7 %all-to-all-start = ((bf16[16,16,256]{2,1,0:T(8,128)(2,1)}), bf16[16,16,256]{2,1,0:T(8,128)(2,1)S(1)}, u32[]{:S(2)}, u32[]{:S(2)}) async-start(bf16[16,16,256]{2,1,0:T(8,128)(2,1)} %broadcast_in_dim.2), calls=%async_computation | async-start | bytes 262144 | tf_op jit(solution)/shard_map/all_to_all | solution.py:30
  25.8 0.7 copy-done.2
  26.5 1.0 prep.1
  27.4 7.6 %all-to-all-done.x_ref = bf16[16,16,256]{2,1,0:T(8,128)(2,1)S(1)} async-done(((bf16[16,16,256]{2,1,0:T(8,128)(2,1)}), bf16[16,16,256]{2,1,0:T(8,128)(2,1)S(1)}, u32[]{:S(2)}, u32[]{:S(2)}) %all-to-all-start) | async-done | bytes 131104 | tf_op jit(solution)/shard_map/all_to_all | solution.py:30
  35.0 0.3 project.1
  35.4 0.8 convert_element_type.27
  36.1 3.6 %all-to-all-start.1 = ((f16[8,160,128]{2,1,0:T(8,128)(2,1)}), f16[8,160,128]{2,1,0:T(8,128)(2,1)S(1)}, u32[]{:S(2)}, u32[]{:S(2)}) async-start(f16[8,160,128]{2,1,0:T(8,128)(2,1)} %convert_element_type.27), calls=%async_computation.1 | async-start | bytes 655360 | tf_op jit(solution)/shard_map/all_to_all | solution.py:30
  39.8 0.8 slice_bitcast_fusion.refs_0_
  40.6 4.3 %collective-permute-start.3 = (bf16[128,256]{1,0:T(8,128)(2,1)S(1)}, bf16[128,256]{1,0:T(8,128)(2,1)S(1)}, u32[]{:S(2)}, u32[]{:S(2)}) collective-permute-start(bf16[128,256]{1,0:T(8,128)(2,1)S(1)} %slice_bitcast_fusion.refs_0_), channel_id=1, source_target_pairs={{5,0},{4,1},{7,2},{6,3},{1,4},{0,5},{3,6},{2,7},{13,8},{12,9},{15,... | collective-permute-start | bytes 196616 | tf_op jit(solution)/shard_map/ppermute | solution.py:101
  44.9 0.3 collective-permute-start.2
  45.2 0.2 collective-permute-start.1
  45.4 2.3 %pack.1.refs_0_ = bf16[272,512]{1,0:T(8,128)(2,1)} custom-call(bf16[2,256]{1,0:T(2,128)(2,1)} %gain_ref.3, bf16[2,256,128]{2,1,0:T(8,128)(2,1)} %wq_ref.1, bf16[2,256,128]{2,1,0:T(8,128)(2,1)} %wf_ref.1, bf16[2,256,128]{2,1,0:T(8,128)(2,1)} %wi_ref.1, bf16[2,256,128]{2,1,0:T(8,128)(2,1)} %wg_ref.1), custom_call_target="tpu_custom_call" | custom-call | tf_op jit(solution)/shard_map/pack/pallas_call | solution.py:54
  47.8 0.0 copy-start
  47.8 4.4 %collective-permute-start.6 = (bf16[272,512]{1,0:T(8,128)(2,1)}, bf16[272,512]{1,0:T(8,128)(2,1)S(1)}, u32[]{:S(2)}, u32[]{:S(2)}) collective-permute-start(bf16[272,512]{1,0:T(8,128)(2,1)} %pack.1.refs_0_), channel_id=1, source_target_pairs={{5,0},{4,1},{7,2},{6,3},{1,4},{0,5},{3,6},{2,7},{13,8},{12,9},{15,... | collective-permute-start | bytes 835592 | tf_op jit(solution)/shard_map/ppermute | solution.py:101
  52.1 0.3 collective-permute-start.5
  52.5 0.0 copy-done.6
  52.5 3.4 %collective-permute-done.3.refs_3_ = bf16[128,256]{1,0:T(8,128)(2,1)S(1)} collective-permute-done((bf16[128,256]{1,0:T(8,128)(2,1)S(1)}, bf16[128,256]{1,0:T(8,128)(2,1)S(1)}, u32[]{:S(2)}, u32[]{:S(2)}) %collective-permute-start.3) | collective-permute-done | bytes 65568 | tf_op jit(solution)/shard_map/ppermute | solution.py:101
  55.8 0.0 collective-permute-start.4
  55.9 0.0 copy-done.5
  55.9 0.1 broadcast_multiply_fusion.shift_ref
  55.9 0.0 all-to-all-done.1
  56.0 0.0 copy-done.4
  56.0 4.0 %first.1 = (f32[2,32,1,128,128]{4,3,2,1,0:T(8,128)}, bf16[64,128]{1,0:T(8,128)(2,1)S(1)}, bf16[64,128]{1,0:T(8,128)(2,1)S(1)}) custom-call(f32[8,160,128]{2,1,0:T(8,128)S(1)} %convert_element_type.28.parts_ref, f32[2,32,128]{2,1,0:T(8,128)S(1)} %broadcast_multiply_fusion.shift_ref, f32[2,128]{1,0:T(2,128)S(1)} %copy-done.3, f32[2,128]{1,0:T(2,128)S(1)} %copy-done.4, ...), custom_call_target="tpu_custom_call" | custom-call | tf_op jit(solution)/shard_map/first/pallas_call | solution.py:278
  60.0 0.0 collective-permute-done.2.refs_2_
  60.1 2.0 %collective-permute-start = (bf16[64,128]{1,0:T(8,128)(2,1)S(1)}, bf16[64,128]{1,0:T(8,128)(2,1)S(1)}, u32[]{:S(2)}, u32[]{:S(2)}) collective-permute-start(bf16[64,128]{1,0:T(8,128)(2,1)S(1)} %get-tuple-element.23), channel_id=1, source_target_pairs={{0,1},{1,0},{2,3},{3,2},{4,5},{5,4},{6,7},{7,6},{8,9},{9,8},{10,11... | collective-permute-start | bytes 49160 | tf_op jit(solution)/shard_map/ppermute | solution.py:106
  62.0 0.0 collective-permute-done.1.refs_1_
  62.0 1.2 collective-permute-done.came_ref
  63.2 0.3 pair.1
  63.5 19.4 %all_to_all.30 = f16[16,32,128]{2,1,0:T(8,128)(2,1)S(1)} all-to-all(f16[16,32,128]{2,1,0:T(8,128)(2,1)S(1)} %convert_element_type.30), channel_id=1, replica_groups=mesh['grp'=2,'tp'=16,'dp'=8] {'tp'}, dimensions={0} | all-to-all | bytes 262144 | tf_op jit(solution)/shard_map/all_to_all | solution.py:30
  83.0 0.0 collective-permute-done.6.refs_3_
  83.0 0.0 collective-permute-done.5.refs_2_
  83.0 0.0 collective-permute-done.4.refs_1_
  83.0 11.6 %all_to_all.31.x_ref = bf16[16,32,128]{2,1,0:T(8,128)(2,1)S(1)} all-to-all(bf16[16,32,128]{2,1,0:T(8,128)(2,1)S(1)} %next.1), channel_id=1, replica_groups=mesh['grp'=2,'tp'=16,'dp'=8] {'tp'}, dimensions={0} | all-to-all | bytes 262144 | tf_op jit(solution)/shard_map/all_to_all | solution.py:30
  94.6 0.5 again.1
  95.1 0.1 collective-permute-start.7
  95.2 1.6 %load.1.prior_ref = f32[32,128,128]{2,1,0:T(8,128)S(1)} custom-call(f32[1,256]{1,0:T(1,128)S(1)} %get-tuple-element.28.gain_ref.ready_ref, f32[2,32,1,128,128]{4,3,2,1,0:T(8,128)} %state_ref.3), custom_call_target="tpu_custom_call" | custom-call | tf_op jit(solution)/shard_map/load/pallas_call | solution.py:175
  96.8 0.0 copy-start.1
  96.8 1.6 %collective-permute-done.7 = f16[32,640]{1,0:T(8,128)(2,1)S(1)} collective-permute-done((f16[32,640]{1,0:T(8,128)(2,1)S(1)}, f16[32,640]{1,0:T(8,128)(2,1)S(1)}, u32[]{:S(2)}, u32[]{:S(2)}) %collective-permute-start.7) | collective-permute-done | bytes 40992 | tf_op jit(solution)/shard_map/ppermute | solution.py:106
  98.5 2.9 %second.1 = (f32[2,32,1,128,128]{4,3,2,1,0:T(8,128)}, bf16[8,40,128]{2,1,0:T(8,128)(2,1)S(1)}) custom-call(f32[32,640]{1,0:T(8,128)S(1)} %get-tuple-element.25.own_ref, f32[32,640]{1,0:T(8,128)S(1)} %convert_element_type.33.came_ref, f32[2,32,128]{2,1,0:T(8,128)S(1)} %broadcast_multiply_fusion.shift_ref, ...), custom_call_target="tpu_custom_call", output_to_operand_aliasing={{0}: (7, {})} | custom-call | tf_op jit(solution)/shard_map/second/pallas_call | solution.py:371
  101.4 13.1 %all_to_all.32.normed_ref = bf16[8,40,128]{2,1,0:T(8,128)(2,1)S(1)} all-to-all(bf16[8,40,128]{2,1,0:T(8,128)(2,1)S(1)} %get-tuple-element.30), channel_id=1, replica_groups=mesh['grp'=2,'tp'=16,'dp'=8] {'dp'}, dimensions={0} | all-to-all | bytes 163840 | tf_op jit(solution)/shard_map/all_to_all | solution.py:30
  114.5 0.3 branch.1
  114.9 13.6 %all_to_all.33 = f16[16,16,256]{2,1,0:T(8,128)(2,1)S(1)} all-to-all(f16[16,16,256]{2,1,0:T(8,128)(2,1)S(1)} %convert_element_type.34), channel_id=1, replica_groups=mesh['grp'=2,'tp'=16,'dp'=8] {'tp'}, dimensions={0} | all-to-all | bytes 262144 | tf_op jit(solution)/shard_map/all_to_all | solution.py:30
  128.6 0.6 final.1
  (13 shorter events, 0.2 us)
Async XLA Ops:
  0.6 51.8 %copy-start.6 = (s32[32]{0:T(128)S(1)}, s32[32]{0:T(128)}, u32[]{:S(2)}) copy-start(s32[32]{0:T(128)} %param.14) | copy-start | bytes 388
  0.6 55.2 %copy-start.5 = (f32[2,128]{1,0:T(2,128)S(1)}, f32[2,128]{1,0:T(2,128)}, u32[]{:S(2)}) copy-start(f32[2,128]{1,0:T(2,128)} %param.22) | copy-start | bytes 3076
  0.7 55.3 %copy-start.4 = (f32[2,128]{1,0:T(2,128)S(1)}, f32[2,128]{1,0:T(2,128)}, u32[]{:S(2)}) copy-start(f32[2,128]{1,0:T(2,128)} %head_ref.3) | copy-start | bytes 3076
  0.7 55.3 %copy-start.3 = (f32[2,128]{1,0:T(2,128)S(1)}, f32[2,128]{1,0:T(2,128)}, u32[]{:S(2)}) copy-start(f32[2,128]{1,0:T(2,128)} %bound_ref.3) | copy-start | bytes 3076
  2.1 33.0 %all-to-all-start = ((bf16[16,16,256]{2,1,0:T(8,128)(2,1)}), bf16[16,16,256]{2,1,0:T(8,128)(2,1)S(1)}, u32[]{:S(2)}, u32[]{:S(2)}) async-start(bf16[16,16,256]{2,1,0:T(8,128)(2,1)} %broadcast_in_dim.2), calls=%async_computation | async-start | bytes 262144 | tf_op jit(solution)/shard_map/all_to_all | solution.py:30
  25.8 0.7 copy-start.2
  36.1 19.8 %all-to-all-start.1 = ((f16[8,160,128]{2,1,0:T(8,128)(2,1)}), f16[8,160,128]{2,1,0:T(8,128)(2,1)S(1)}, u32[]{:S(2)}, u32[]{:S(2)}) async-start(f16[8,160,128]{2,1,0:T(8,128)(2,1)} %convert_element_type.27), calls=%async_computation.1 | async-start | bytes 655360 | tf_op jit(solution)/shard_map/all_to_all | solution.py:30
  40.6 15.2 %collective-permute-start.3 = (bf16[128,256]{1,0:T(8,128)(2,1)S(1)}, bf16[128,256]{1,0:T(8,128)(2,1)S(1)}, u32[]{:S(2)}, u32[]{:S(2)}) collective-permute-start(bf16[128,256]{1,0:T(8,128)(2,1)S(1)} %slice_bitcast_fusion.refs_0_), channel_id=1, source_target_pairs={{5,0},{4,1},{7,2},{6,3},{1,4},{0,5},{3,6},{2,7},{13,8},{12,9},{15,... | collective-permute-start | bytes 196616 | tf_op jit(solution)/shard_map/ppermute | solution.py:101
  44.9 15.2 %collective-permute-start.2 = (bf16[128,256]{1,0:T(8,128)(2,1)S(1)}, bf16[128,256]{1,0:T(8,128)(2,1)S(1)}, u32[]{:S(2)}, u32[]{:S(2)}) collective-permute-start(bf16[128,256]{1,0:T(8,128)(2,1)S(1)} %slice_bitcast_fusion.refs_0_), channel_id=1, source_target_pairs={{6,0},{3,1},{0,2},{5,3},{2,4},{7,5},{4,6},{1,7},{14,8},{11,9},{8,1... | collective-permute-start | bytes 196616 | tf_op jit(solution)/shard_map/ppermute | solution.py:101
  45.2 16.8 %collective-permute-start.1 = (bf16[128,256]{1,0:T(8,128)(2,1)S(1)}, bf16[128,256]{1,0:T(8,128)(2,1)S(1)}, u32[]{:S(2)}, u32[]{:S(2)}) collective-permute-start(bf16[128,256]{1,0:T(8,128)(2,1)S(1)} %slice_bitcast_fusion.refs_0_), channel_id=1, source_target_pairs={{7,0},{2,1},{1,2},{4,3},{3,4},{6,5},{5,6},{0,7},{15,8},{10,9},{9,1... | collective-permute-start | bytes 196616 | tf_op jit(solution)/shard_map/ppermute | solution.py:101
  47.8 46.8 %copy-start = (bf16[272,512]{1,0:T(8,128)(2,1)S(1)}, bf16[272,512]{1,0:T(8,128)(2,1)}, u32[]{:S(2)}) copy-start(bf16[272,512]{1,0:T(8,128)(2,1)} %pack.1.refs_0_) | copy-start | bytes 835588
  47.8 35.2 %collective-permute-start.6 = (bf16[272,512]{1,0:T(8,128)(2,1)}, bf16[272,512]{1,0:T(8,128)(2,1)S(1)}, u32[]{:S(2)}, u32[]{:S(2)}) collective-permute-start(bf16[272,512]{1,0:T(8,128)(2,1)} %pack.1.refs_0_), channel_id=1, source_target_pairs={{5,0},{4,1},{7,2},{6,3},{1,4},{0,5},{3,6},{2,7},{13,8},{12,9},{15,... | collective-permute-start | bytes 835592 | tf_op jit(solution)/shard_map/ppermute | solution.py:101
  52.1 30.8 %collective-permute-start.5 = (bf16[272,512]{1,0:T(8,128)(2,1)}, bf16[272,512]{1,0:T(8,128)(2,1)S(1)}, u32[]{:S(2)}, u32[]{:S(2)}) collective-permute-start(bf16[272,512]{1,0:T(8,128)(2,1)} %pack.1.refs_0_), channel_id=1, source_target_pairs={{6,0},{3,1},{0,2},{5,3},{2,4},{7,5},{4,6},{1,7},{14,8},{11,9},{8,1... | collective-permute-start | bytes 835592 | tf_op jit(solution)/shard_map/ppermute | solution.py:101
  55.8 27.1 %collective-permute-start.4 = (bf16[272,512]{1,0:T(8,128)(2,1)}, bf16[272,512]{1,0:T(8,128)(2,1)S(1)}, u32[]{:S(2)}, u32[]{:S(2)}) collective-permute-start(bf16[272,512]{1,0:T(8,128)(2,1)} %pack.1.refs_0_), channel_id=1, source_target_pairs={{7,0},{2,1},{1,2},{4,3},{3,4},{6,5},{5,6},{0,7},{15,8},{10,9},{9,1... | collective-permute-start | bytes 835592 | tf_op jit(solution)/shard_map/ppermute | solution.py:101
  60.1 3.1 %collective-permute-start = (bf16[64,128]{1,0:T(8,128)(2,1)S(1)}, bf16[64,128]{1,0:T(8,128)(2,1)S(1)}, u32[]{:S(2)}, u32[]{:S(2)}) collective-permute-start(bf16[64,128]{1,0:T(8,128)(2,1)S(1)} %get-tuple-element.23), channel_id=1, source_target_pairs={{0,1},{1,0},{2,3},{3,2},{4,5},{5,4},{6,7},{7,6},{8,9},{9,8},{10,11... | collective-permute-start | bytes 49160 | tf_op jit(solution)/shard_map/ppermute | solution.py:106
  95.1 3.4 %collective-permute-start.7 = (f16[32,640]{1,0:T(8,128)(2,1)S(1)}, f16[32,640]{1,0:T(8,128)(2,1)S(1)}, u32[]{:S(2)}, u32[]{:S(2)}) collective-permute-start(f16[32,640]{1,0:T(8,128)(2,1)S(1)} %convert_element_type.32), channel_id=1, source_target_pairs={{0,1},{1,0},{2,3},{3,2},{4,5},{5,4},{6,7},{7,6},{8,9},{9,8},{10,11... | collective-permute-start | bytes 122888 | tf_op jit(solution)/shard_map/ppermute | solution.py:106
  96.8 17.7 %copy-start.1 = (bf16[2,128,256]{2,1,0:T(8,128)(2,1)S(1)}, bf16[2,128,256]{2,1,0:T(8,128)(2,1)}, u32[]{:S(2)}) copy-start(bf16[2,128,256]{2,1,0:T(8,128)(2,1)} %w_ref.1) | copy-start | bytes 393220

commit v5 on v4

--- a/solution.py
+++ b/solution.py
@@ -123,6 +123,21 @@
     return jnp.where(total < 0.0, -root, root)
 
 
+def packed_rows(block):
+    size = block.shape[1]
+    count = block.shape[0] * LANES // size
+    total = block[:count]
+    for group in range(1, size // LANES):
+        total += pltpu.roll(block[group * count : (group + 1) * count], group * LANES, 1)
+    return total
+
+
+def unpacked_rows(block):
+    size = block.shape[1]
+    groups = [block] + [pltpu.roll(block, size - group * LANES, 1) for group in range(1, size // LANES)]
+    return jnp.concatenate(groups, axis=0)
+
+
 def scaled(squares, bits):
     power = jnp.ceil(0.5 * jnp.log2(jnp.maximum(squares, FLOOR)))
     down = jnp.exp2(-power)
@@ -133,7 +148,7 @@
 
 def project_kernel(share, x_ref, gain_ref, wq_ref, wf_ref, wi_ref, wg_ref, out_ref):
     owners, size = out_ref.shape[0], out_ref.shape[-1]
-    rows = out_ref.shape[1] // 5
+    rows = x_ref.shape[0] * x_ref.shape[1] // owners
     held = x_ref[...].reshape(owners * rows, x_ref.shape[-1])
     x = held.astype(jnp.float32)
     squares = jnp.sum(x * x, axis=1, keepdims=True)
@@ -150,15 +165,18 @@
     table = jnp.where(lane == 0, power - 13.0, jnp.where(lane == 1, high, jnp.where(lane == 2, mantissa - high, 0.0)))
     choose = selection(held.shape[1], size, lax.axis_index("tp") * share, SHARE_AT, share)
     kept = factor * jnp.dot(held, choose, preferred_element_type=jnp.float32)
-    out_ref[:, 4 * rows :, :] = (table + kept).reshape(owners, rows, size)
+    both = table + kept
+    for owner in range(owners):
+        out_ref[owner, 4 * rows :, :] = packed_rows(both[owner * rows : (owner + 1) * rows])
 
 
 def project(whole, gain, weights, owners):
     rows = whole.shape[0] * whole.shape[1] // owners
     share = whole.shape[2] // lax.axis_size("tp")
+    extra = rows * LANES // weights[0].shape[1]
     return pl.pallas_call(
         functools.partial(project_kernel, share),
-        out_shape=jax.ShapeDtypeStruct((owners, 5 * rows, weights[0].shape[1]), jnp.float32),
+        out_shape=jax.ShapeDtypeStruct((owners, 4 * rows + extra, weights[0].shape[1]), jnp.float32),
         compiler_params=PARAMS,
         name="project",
     )(whole, gain, *weights)
@@ -219,7 +237,7 @@
     count = shift_ref.shape[1]
     made, squares = [0.0] * 4, 0.0
     for source in range(owners):
-        table = parts_ref[source, 4 * count :, :]
+        table = unpacked_rows(parts_ref[source, 4 * count :, :])
         up = jnp.exp2(table[:, 0:1])
         norm = up * 2.0**13
         squares += (table[:, 1:2] + table[:, 2:3]) * norm * norm
@@ -232,7 +250,7 @@
     for out_ref, holder in ((own_ref, device), (sent_ref, neighbour)):
         kept = 0.0
         for n in range(owners // 2):
-            table = parts_ref[near_chunk(n, owners, holder), 4 * count :, :]
+            table = unpacked_rows(parts_ref[near_chunk(n, owners, holder), 4 * count :, :])
             place = selection(size, size, SHARE_AT, n * LANES, share)
             moved = jnp.dot(table.astype(jnp.bfloat16), place, preferred_element_type=jnp.float32)
             kept += jnp.exp2(table[:, 0:1]) * moved
@@ -298,7 +316,7 @@
 
 def again_kernel(share, x_ref, *refs):
     shards, (own_ref, sent_ref, kept_ref) = refs[:-3], refs[-3:]
-    owners, packed, size = kept_ref.shape
+    owners, _, size = kept_ref.shape
     count = x_ref.shape[1]
     rows = shards[0].shape[0] - PAD
     parts = rows // size
@@ -319,10 +337,7 @@
         made += jnp.dot(gained, shard[:rows, :], preferred_element_type=jnp.float32)
         kept = [jnp.dot(halves[half], choose[half], preferred_element_type=jnp.float32) for half in range(2)]
         kept = kept[0] + kept[1]
-        block = kept[:packed]
-        for group in range(1, count // packed):
-            block += pltpu.roll(kept[group * packed : (group + 1) * packed], group * LANES, 1)
-        kept_ref[near_chunk(n, owners)] = block.astype(kept_ref.dtype)
+        kept_ref[near_chunk(n, owners)] = packed_rows(kept).astype(kept_ref.dtype)
     own_ref[:, : made.shape[1]] = made[:count]
     own_ref[:, made.shape[1] :] = jnp.broadcast_to(squares[:count], (count, size))
     factor, columns = scaled(squares[count:], 12)

time: 130 us -> 129 us (level)
  blocking collectives: 57.7 us -> 55.9 us
    all_to_all x4, blocking collectives: 57.7 us -> 55.9 us  [exchange(): return lax.all_to_all(x, axis, split_axis=0, concat_axis=0, tiled=True)]
  transfers between devices with their start and end apart: 10 -> 10, of which waited for: 4 -> 5; matrix products, arithmetic and copies ran while one was open for 1% -> 1% of each run, Pallas kernels for 7% -> 7%
where the time goes in v5:
time: 129 us; the launch traced here: 128 us
  blocking collectives  55.9 us (43%)
  starting transfers between devices  39.9 us (31%)
  Pallas kernels  14.2 us (11%)
  waiting for transfers between devices  13.5 us (10%)
  local copies, waits for them, and re-layouts  2.93 us (2%)
    all_to_all x4, blocking collectives, exchange(): return lax.all_to_all(x, axis, split_axis=0, concat_axis=0, tiled=True)  55.9 us
    all_to_all x2, starting transfers between devices, exchange(): return lax.all_to_all(x, axis, split_axis=0, concat_axis=0, tiled=True)  27.3 us
    ppermute x6, starting transfers between devices, near(): held.append(lax.ppermute(shard, axis, pairs))  9.46 us
    all_to_all x2, waiting for transfers between devices, exchange(): return lax.all_to_all(x, axis, split_axis=0, concat_axis=0, tiled=True)  7.6 us
    pallas_call x1, Pallas kernels, first(): pl.pallas_call(functools.partial(first_kernel, share), in_specs=[VMEM] *...  4.18 us
    ppermute x2, starting transfers between devices, swap(): lax.ppermute(x, axis, [(n, n ^ 1) for n in range(lax.axis_size(axis))])  3.1 us
    ppermute x2, waiting for transfers between devices, swap(): lax.ppermute(x, axis, [(n, n ^ 1) for n in range(lax.axis_size(axis))])  3.08 us
    pallas_call x1, Pallas kernels, second(): pl.pallas_call(second_kernel, in_specs=[VMEM] * 7 + [HBM], out_specs=[HBM...  2.93 us
  transfers between devices with their start and end apart: 10, of which 5 were waited for; matrix products, arithmetic and copies ran while one was open for 1% of the time, Pallas kernels for 7%

profile of v5, /device:TPU:513, one launch (start us, length us, event | category | flops | bytes accessed | tf_op | source)
XLA Modules:
  0.0 128.2 jit_solution(3673955858101981224)
XLA Ops:
  0.6 0.0 copy-start.6
  0.6 0.0 copy-start.5
  0.7 0.0 copy-start.4
  0.7 0.0 copy-start.3
  0.7 1.4 %broadcast_in_dim.2 = bf16[16,16,256]{2,1,0:T(8,128)(2,1)} broadcast(bf16[16,256]{1,0:T(8,128)(2,1)} %param.12), dimensions={1,2} | broadcast | bytes 139264 | tf_op jit(solution)/shard_map/broadcast_in_dim | solution.py:449
  2.1 23.7 %all-to-all-start = ((bf16[16,16,256]{2,1,0:T(8,128)(2,1)}), bf16[16,16,256]{2,1,0:T(8,128)(2,1)S(1)}, u32[]{:S(2)}, u32[]{:S(2)}) async-start(bf16[16,16,256]{2,1,0:T(8,128)(2,1)} %broadcast_in_dim.2), calls=%async_computation | async-start | bytes 262144 | tf_op jit(solution)/shard_map/all_to_all | solution.py:30
  25.8 0.7 copy-done.2
  26.5 1.0 prep.1
  27.4 7.6 %all-to-all-done.x_ref = bf16[16,16,256]{2,1,0:T(8,128)(2,1)S(1)} async-done(((bf16[16,16,256]{2,1,0:T(8,128)(2,1)}), bf16[16,16,256]{2,1,0:T(8,128)(2,1)S(1)}, u32[]{:S(2)}, u32[]{:S(2)}) %all-to-all-start) | async-done | bytes 131104 | tf_op jit(solution)/shard_map/all_to_all | solution.py:30
  35.0 0.4 project.1
  35.4 0.8 convert_element_type.27
  36.2 3.6 %all-to-all-start.1 = ((f16[8,136,128]{2,1,0:T(8,128)(2,1)}), f16[8,136,128]{2,1,0:T(8,128)(2,1)S(1)}, u32[]{:S(2)}, u32[]{:S(2)}) async-start(f16[8,136,128]{2,1,0:T(8,128)(2,1)} %convert_element_type.27), calls=%async_computation.1 | async-start | bytes 557056 | tf_op jit(solution)/shard_map/all_to_all | solution.py:30
  39.8 0.8 slice_bitcast_fusion.refs_0_
  40.7 4.3 %collective-permute-start.3 = (bf16[128,256]{1,0:T(8,128)(2,1)S(1)}, bf16[128,256]{1,0:T(8,128)(2,1)S(1)}, u32[]{:S(2)}, u32[]{:S(2)}) collective-permute-start(bf16[128,256]{1,0:T(8,128)(2,1)S(1)} %slice_bitcast_fusion.refs_0_), channel_id=1, source_target_pairs={{5,0},{4,1},{7,2},{6,3},{1,4},{0,5},{3,6},{2,7},{13,8},{12,9},{15,... | collective-permute-start | bytes 196616 | tf_op jit(solution)/shard_map/ppermute | solution.py:101
  44.9 0.3 collective-permute-start.2
  45.2 0.2 collective-permute-start.1
  45.4 2.3 %pack.1.refs_0_ = bf16[272,512]{1,0:T(8,128)(2,1)} custom-call(bf16[2,256]{1,0:T(2,128)(2,1)} %gain_ref.3, bf16[2,256,128]{2,1,0:T(8,128)(2,1)} %wq_ref.1, bf16[2,256,128]{2,1,0:T(8,128)(2,1)} %wf_ref.1, bf16[2,256,128]{2,1,0:T(8,128)(2,1)} %wi_ref.1, bf16[2,256,128]{2,1,0:T(8,128)(2,1)} %wg_ref.1), custom_call_target="tpu_custom_call" | custom-call | tf_op jit(solution)/shard_map/pack/pallas_call | solution.py:54
  47.8 0.0 copy-start
  47.8 4.4 %collective-permute-start.6 = (bf16[272,512]{1,0:T(8,128)(2,1)}, bf16[272,512]{1,0:T(8,128)(2,1)S(1)}, u32[]{:S(2)}, u32[]{:S(2)}) collective-permute-start(bf16[272,512]{1,0:T(8,128)(2,1)} %pack.1.refs_0_), channel_id=1, source_target_pairs={{5,0},{4,1},{7,2},{6,3},{1,4},{0,5},{3,6},{2,7},{13,8},{12,9},{15,... | collective-permute-start | bytes 835592 | tf_op jit(solution)/shard_map/ppermute | solution.py:101
  52.2 0.3 collective-permute-start.5
  52.5 0.0 copy-done.6
  52.5 1.8 %collective-permute-done.3.refs_3_ = bf16[128,256]{1,0:T(8,128)(2,1)S(1)} collective-permute-done((bf16[128,256]{1,0:T(8,128)(2,1)S(1)}, bf16[128,256]{1,0:T(8,128)(2,1)S(1)}, u32[]{:S(2)}, u32[]{:S(2)}) %collective-permute-start.3) | collective-permute-done | bytes 65568 | tf_op jit(solution)/shard_map/ppermute | solution.py:101
  54.3 0.0 collective-permute-start.4
  54.3 0.0 copy-done.5
  54.3 0.1 broadcast_multiply_fusion.shift_ref
  54.4 0.0 all-to-all-done.1
  54.4 0.0 copy-done.4
  54.4 4.2 %first.1 = (f32[2,32,1,128,128]{4,3,2,1,0:T(8,128)}, bf16[64,128]{1,0:T(8,128)(2,1)S(1)}, bf16[64,128]{1,0:T(8,128)(2,1)S(1)}) custom-call(f32[8,136,128]{2,1,0:T(8,128)S(1)} %convert_element_type.28.parts_ref, f32[2,32,128]{2,1,0:T(8,128)S(1)} %broadcast_multiply_fusion.shift_ref, f32[2,128]{1,0:T(2,128)S(1)} %copy-done.3, f32[2,128]{1,0:T(2,128)S(1)} %copy-done.4, ...), custom_call_target="tpu_custom_call" | custom-call | tf_op jit(solution)/shard_map/first/pallas_call | solution.py:296
  58.6 0.0 collective-permute-done.2.refs_2_
  58.6 2.6 %collective-permute-start = (bf16[64,128]{1,0:T(8,128)(2,1)S(1)}, bf16[64,128]{1,0:T(8,128)(2,1)S(1)}, u32[]{:S(2)}, u32[]{:S(2)}) collective-permute-start(bf16[64,128]{1,0:T(8,128)(2,1)S(1)} %get-tuple-element.23), channel_id=1, source_target_pairs={{0,1},{1,0},{2,3},{3,2},{4,5},{5,4},{6,7},{7,6},{8,9},{9,8},{10,11... | collective-permute-start | bytes 49160 | tf_op jit(solution)/shard_map/ppermute | solution.py:106
  61.2 0.0 collective-permute-done.1.refs_1_
  61.2 1.4 %collective-permute-done.came_ref = bf16[64,128]{1,0:T(8,128)(2,1)S(1)} collective-permute-done((bf16[64,128]{1,0:T(8,128)(2,1)S(1)}, bf16[64,128]{1,0:T(8,128)(2,1)S(1)}, u32[]{:S(2)}, u32[]{:S(2)}) %collective-permute-start) | collective-permute-done | bytes 16416 | tf_op jit(solution)/shard_map/ppermute | solution.py:106
  62.7 0.3 pair.1
  63.0 15.0 %all_to_all.30 = f16[16,32,128]{2,1,0:T(8,128)(2,1)S(1)} all-to-all(f16[16,32,128]{2,1,0:T(8,128)(2,1)S(1)} %convert_element_type.30), channel_id=1, replica_groups=mesh['grp'=2,'tp'=16,'dp'=8] {'tp'}, dimensions={0} | all-to-all | bytes 262144 | tf_op jit(solution)/shard_map/all_to_all | solution.py:30
  78.1 0.0 collective-permute-done.6.refs_3_
  78.1 0.0 collective-permute-done.5.refs_2_
  78.1 1.0 collective-permute-done.4.refs_1_
  79.1 12.2 %all_to_all.31.x_ref = bf16[16,32,128]{2,1,0:T(8,128)(2,1)S(1)} all-to-all(bf16[16,32,128]{2,1,0:T(8,128)(2,1)S(1)} %next.1), channel_id=1, replica_groups=mesh['grp'=2,'tp'=16,'dp'=8] {'tp'}, dimensions={0} | all-to-all | bytes 262144 | tf_op jit(solution)/shard_map/all_to_all | solution.py:30
  91.3 0.5 again.1
  91.8 0.5 collective-permute-start.7
  92.3 1.6 %load.1.prior_ref = f32[32,128,128]{2,1,0:T(8,128)S(1)} custom-call(f32[1,256]{1,0:T(1,128)S(1)} %get-tuple-element.28.gain_ref.ready_ref, f32[2,32,1,128,128]{4,3,2,1,0:T(8,128)} %state_ref.3), custom_call_target="tpu_custom_call" | custom-call | tf_op jit(solution)/shard_map/load/pallas_call | solution.py:193
  93.9 0.0 copy-start.1
  93.9 1.6 %collective-permute-done.7 = f16[32,640]{1,0:T(8,128)(2,1)S(1)} collective-permute-done((f16[32,640]{1,0:T(8,128)(2,1)S(1)}, f16[32,640]{1,0:T(8,128)(2,1)S(1)}, u32[]{:S(2)}, u32[]{:S(2)}) %collective-permute-start.7) | collective-permute-done | bytes 40992 | tf_op jit(solution)/shard_map/ppermute | solution.py:106
  95.6 2.9 %second.1 = (f32[2,32,1,128,128]{4,3,2,1,0:T(8,128)}, bf16[8,40,128]{2,1,0:T(8,128)(2,1)S(1)}) custom-call(f32[32,640]{1,0:T(8,128)S(1)} %get-tuple-element.25.own_ref, f32[32,640]{1,0:T(8,128)S(1)} %convert_element_type.33.came_ref, f32[2,32,128]{2,1,0:T(8,128)S(1)} %broadcast_multiply_fusion.shift_ref, ...), custom_call_target="tpu_custom_call", output_to_operand_aliasing={{0}: (7, {})} | custom-call | tf_op jit(solution)/shard_map/second/pallas_call | solution.py:386
  98.5 15.0 %all_to_all.32.normed_ref = bf16[8,40,128]{2,1,0:T(8,128)(2,1)S(1)} all-to-all(bf16[8,40,128]{2,1,0:T(8,128)(2,1)S(1)} %get-tuple-element.30), channel_id=1, replica_groups=mesh['grp'=2,'tp'=16,'dp'=8] {'dp'}, dimensions={0} | all-to-all | bytes 163840 | tf_op jit(solution)/shard_map/all_to_all | solution.py:30
  113.5 0.3 branch.1
  113.9 13.6 %all_to_all.33 = f16[16,16,256]{2,1,0:T(8,128)(2,1)S(1)} all-to-all(f16[16,16,256]{2,1,0:T(8,128)(2,1)S(1)} %convert_element_type.34), channel_id=1, replica_groups=mesh['grp'=2,'tp'=16,'dp'=8] {'tp'}, dimensions={0} | all-to-all | bytes 262144 | tf_op jit(solution)/shard_map/all_to_all | solution.py:30
  127.5 0.6 final.1
  (13 shorter events, 0.2 us)
Async XLA Ops:
  0.6 51.9 %copy-start.6 = (s32[32]{0:T(128)S(1)}, s32[32]{0:T(128)}, u32[]{:S(2)}) copy-start(s32[32]{0:T(128)} %param.14) | copy-start | bytes 388
  0.6 53.6 %copy-start.5 = (f32[2,128]{1,0:T(2,128)S(1)}, f32[2,128]{1,0:T(2,128)}, u32[]{:S(2)}) copy-start(f32[2,128]{1,0:T(2,128)} %param.22) | copy-start | bytes 3076
  0.7 53.8 %copy-start.4 = (f32[2,128]{1,0:T(2,128)S(1)}, f32[2,128]{1,0:T(2,128)}, u32[]{:S(2)}) copy-start(f32[2,128]{1,0:T(2,128)} %head_ref.3) | copy-start | bytes 3076
  0.7 53.8 %copy-start.3 = (f32[2,128]{1,0:T(2,128)S(1)}, f32[2,128]{1,0:T(2,128)}, u32[]{:S(2)}) copy-start(f32[2,128]{1,0:T(2,128)} %bound_ref.3) | copy-start | bytes 3076
  2.1 33.0 %all-to-all-start = ((bf16[16,16,256]{2,1,0:T(8,128)(2,1)}), bf16[16,16,256]{2,1,0:T(8,128)(2,1)S(1)}, u32[]{:S(2)}, u32[]{:S(2)}) async-start(bf16[16,16,256]{2,1,0:T(8,128)(2,1)} %broadcast_in_dim.2), calls=%async_computation | async-start | bytes 262144 | tf_op jit(solution)/shard_map/all_to_all | solution.py:30
  25.8 0.7 copy-start.2
  36.2 18.2 %all-to-all-start.1 = ((f16[8,136,128]{2,1,0:T(8,128)(2,1)}), f16[8,136,128]{2,1,0:T(8,128)(2,1)S(1)}, u32[]{:S(2)}, u32[]{:S(2)}) async-start(f16[8,136,128]{2,1,0:T(8,128)(2,1)} %convert_element_type.27), calls=%async_computation.1 | async-start | bytes 557056 | tf_op jit(solution)/shard_map/all_to_all | solution.py:30
  40.7 13.6 %collective-permute-start.3 = (bf16[128,256]{1,0:T(8,128)(2,1)S(1)}, bf16[128,256]{1,0:T(8,128)(2,1)S(1)}, u32[]{:S(2)}, u32[]{:S(2)}) collective-permute-start(bf16[128,256]{1,0:T(8,128)(2,1)S(1)} %slice_bitcast_fusion.refs_0_), channel_id=1, source_target_pairs={{5,0},{4,1},{7,2},{6,3},{1,4},{0,5},{3,6},{2,7},{13,8},{12,9},{15,... | collective-permute-start | bytes 196616 | tf_op jit(solution)/shard_map/ppermute | solution.py:101
  44.9 13.7 %collective-permute-start.2 = (bf16[128,256]{1,0:T(8,128)(2,1)S(1)}, bf16[128,256]{1,0:T(8,128)(2,1)S(1)}, u32[]{:S(2)}, u32[]{:S(2)}) collective-permute-start(bf16[128,256]{1,0:T(8,128)(2,1)S(1)} %slice_bitcast_fusion.refs_0_), channel_id=1, source_target_pairs={{6,0},{3,1},{0,2},{5,3},{2,4},{7,5},{4,6},{1,7},{14,8},{11,9},{8,1... | collective-permute-start | bytes 196616 | tf_op jit(solution)/shard_map/ppermute | solution.py:101
  45.2 16.0 %collective-permute-start.1 = (bf16[128,256]{1,0:T(8,128)(2,1)S(1)}, bf16[128,256]{1,0:T(8,128)(2,1)S(1)}, u32[]{:S(2)}, u32[]{:S(2)}) collective-permute-start(bf16[128,256]{1,0:T(8,128)(2,1)S(1)} %slice_bitcast_fusion.refs_0_), channel_id=1, source_target_pairs={{7,0},{2,1},{1,2},{4,3},{3,4},{6,5},{5,6},{0,7},{15,8},{10,9},{9,1... | collective-permute-start | bytes 196616 | tf_op jit(solution)/shard_map/ppermute | solution.py:101
  47.8 43.5 %copy-start = (bf16[272,512]{1,0:T(8,128)(2,1)S(1)}, bf16[272,512]{1,0:T(8,128)(2,1)}, u32[]{:S(2)}) copy-start(bf16[272,512]{1,0:T(8,128)(2,1)} %pack.1.refs_0_) | copy-start | bytes 835588
  47.8 30.3 %collective-permute-start.6 = (bf16[272,512]{1,0:T(8,128)(2,1)}, bf16[272,512]{1,0:T(8,128)(2,1)S(1)}, u32[]{:S(2)}, u32[]{:S(2)}) collective-permute-start(bf16[272,512]{1,0:T(8,128)(2,1)} %pack.1.refs_0_), channel_id=1, source_target_pairs={{5,0},{4,1},{7,2},{6,3},{1,4},{0,5},{3,6},{2,7},{13,8},{12,9},{15,... | collective-permute-start | bytes 835592 | tf_op jit(solution)/shard_map/ppermute | solution.py:101
  52.2 25.9 %collective-permute-start.5 = (bf16[272,512]{1,0:T(8,128)(2,1)}, bf16[272,512]{1,0:T(8,128)(2,1)S(1)}, u32[]{:S(2)}, u32[]{:S(2)}) collective-permute-start(bf16[272,512]{1,0:T(8,128)(2,1)} %pack.1.refs_0_), channel_id=1, source_target_pairs={{6,0},{3,1},{0,2},{5,3},{2,4},{7,5},{4,6},{1,7},{14,8},{11,9},{8,1... | collective-permute-start | bytes 835592 | tf_op jit(solution)/shard_map/ppermute | solution.py:101
  54.3 24.8 %collective-permute-start.4 = (bf16[272,512]{1,0:T(8,128)(2,1)}, bf16[272,512]{1,0:T(8,128)(2,1)S(1)}, u32[]{:S(2)}, u32[]{:S(2)}) collective-permute-start(bf16[272,512]{1,0:T(8,128)(2,1)} %pack.1.refs_0_), channel_id=1, source_target_pairs={{7,0},{2,1},{1,2},{4,3},{3,4},{6,5},{5,6},{0,7},{15,8},{10,9},{9,1... | collective-permute-start | bytes 835592 | tf_op jit(solution)/shard_map/ppermute | solution.py:101
  58.6 4.0 %collective-permute-start = (bf16[64,128]{1,0:T(8,128)(2,1)S(1)}, bf16[64,128]{1,0:T(8,128)(2,1)S(1)}, u32[]{:S(2)}, u32[]{:S(2)}) collective-permute-start(bf16[64,128]{1,0:T(8,128)(2,1)S(1)} %get-tuple-element.23), channel_id=1, source_target_pairs={{0,1},{1,0},{2,3},{3,2},{4,5},{5,4},{6,7},{7,6},{8,9},{9,8},{10,11... | collective-permute-start | bytes 49160 | tf_op jit(solution)/shard_map/ppermute | solution.py:106
  91.8 3.8 %collective-permute-start.7 = (f16[32,640]{1,0:T(8,128)(2,1)S(1)}, f16[32,640]{1,0:T(8,128)(2,1)S(1)}, u32[]{:S(2)}, u32[]{:S(2)}) collective-permute-start(f16[32,640]{1,0:T(8,128)(2,1)S(1)} %convert_element_type.32), channel_id=1, source_target_pairs={{0,1},{1,0},{2,3},{3,2},{4,5},{5,4},{6,7},{7,6},{8,9},{9,8},{10,11... | collective-permute-start | bytes 122888 | tf_op jit(solution)/shard_map/ppermute | solution.py:106
  93.9 19.6 %copy-start.1 = (bf16[2,128,256]{2,1,0:T(8,128)(2,1)S(1)}, bf16[2,128,256]{2,1,0:T(8,128)(2,1)}, u32[]{:S(2)}) copy-start(bf16[2,128,256]{2,1,0:T(8,128)(2,1)} %w_ref.1) | copy-start | bytes 393220
